TPU v7x, 256 devices: a whole 4x4x8 slice. The times are simulated.
256 devices in a mesh: sp: 32 (over z, x), tp: 8 (over y, core).
Axes of the slice: x: 4, y: 4, z: 8, core: 2. Of those that a mesh axis runs over, the one named last changes fastest.
Arguments:
- tokens_in: bfloat16 [16384, 4096], P(('sp', 'tp')), may hold values from -64 to 64
- w_query: bfloat16 [4096, 2048], P(None, 'tp'), may hold values from -0.09375 to 0.09375
- w_key: bfloat16 [4096, 2048], P(None, 'tp'), may hold values from -0.09375 to 0.09375
- w_value: bfloat16 [4096, 2048], P(None, 'tp'), may hold values from -0.09375 to 0.09375
- w_out: bfloat16 [2048, 4096], P('tp'), may hold values from -1 to 1
Outputs:
- mixed: bfloat16 [16384, 4096], P(('sp', 'tp'))
- log_weight: float32 [32, 16384], P('tp', 'sp')
All inputs are finite; a program needn't handle non-finite values.
Results may differ from a plain program's by a relative error of at most 0.019.
Values may be sent and summed in bfloat16 or wider, within the bound.
A program may use at most 128 MiB of HBM per device.

v0:
```python
import functools

import jax
import jax.numpy as jnp
import numpy as np
from jax import lax
from jax.experimental import pallas as pl
from jax.experimental.pallas import tpu as pltpu
from jax.sharding import PartitionSpec as P

NZ, NX, NY = 8, 4, 4
SHARD = 64
ROWS = 512
D = 4096
COLS = 256
HALF = D // 2
SIDE = 64
TOKENS = 16384
ROTARY_BASE = 500000.0
NEG = -1e30
MESH = pl.DeviceIdType.MESH
BF = jnp.bfloat16
F32 = jnp.float32
NT = (((1,), (1,)), ((), ()))


def rotary_tables():
    lane = np.arange(128)
    freq = ROTARY_BASE ** (-(lane % 32) / 32.0)
    sign = np.where(lane % 64 < 32, -1.0, 1.0)
    near = np.arange(SHARD)[:, None] * freq[None, :]
    far = (np.arange(TOKENS // SHARD) * SHARD)[:, None] * freq[None, :]
    near = np.stack([np.cos(near), sign * np.sin(near)])
    far = np.stack([np.cos(far), sign * np.sin(far)])
    return near.astype(np.float32), far.astype(np.float32)


def iota(shape, dim):
    return lax.broadcasted_iota(jnp.int32, shape, dim)


def head_lanes(width=COLS):
    return iota((1, width), 1) // 64


def attend(q, k, v, bias):
    rows = q.shape[0]
    lanes = head_lanes()
    stacked = jnp.concatenate([q * (lanes == h).astype(F32).astype(BF) for h in range(4)], axis=0)
    scores = lax.dot_general(stacked, k, NT, preferred_element_type=F32)
    scores = scores + jnp.concatenate([bias] * 4, axis=0)
    top = jnp.max(scores, axis=1, keepdims=True)
    expo = jnp.exp(scores - top)
    total = jnp.sum(expo, axis=1, keepdims=True)
    out = jnp.dot(expo.astype(BF), v, preferred_element_type=F32) / total
    lse = top + jnp.log(total)
    small = iota((1, 128), 1)
    merged = jnp.zeros((rows, COLS), F32)
    sums = jnp.zeros((rows, 128), F32)
    for h in range(4):
        part = slice(h * rows, (h + 1) * rows)
        merged = jnp.where(lanes == h, out[part], merged)
        sums = jnp.where(small == h, lse[part], sums)
    return merged, sums


def merge(out_a, lse_a, out_b, lse_b):
    peak = jnp.maximum(lse_a, lse_b)
    share_a = jnp.exp(lse_a - peak)
    share_b = jnp.exp(lse_b - peak)
    total = share_a + share_b
    lanes = head_lanes()
    wide_a = jnp.zeros(out_a.shape, F32)
    wide_b = jnp.zeros(out_a.shape, F32)
    share_a = share_a / total
    share_b = share_b / total
    for h in range(4):
        wide_a = jnp.where(lanes == h, share_a[:, h : h + 1], wide_a)
        wide_b = jnp.where(lanes == h, share_b[:, h : h + 1], wide_b)
    return wide_a * out_a + wide_b * out_b, peak + jnp.log(total)


def kernel(
    x_hbm, wq_hbm, wk_hbm, wv_hbm, wo_hbm, near_hbm, far_hbm,
    mixed_ref, logw_ref,
    xbuf, w, wo, near, far,
    rot, qn, kvn, send_q, send_kv, qa, kv5, qb, kvb,
    bias1, bias8, bias64,
    o8, l8, ob, lb, ro, rl, rlt, ri, rit, o1, l1, o2, l2,
    att, rb, rv,
    loc_sem, ag_send, ag_recv, dd_send, dd_recv, wo_send, wo_recv,
    xs_send, xs_recv, z_send, z_recv, n_send, n_recv, ret_send, ret_recv,
    at_send, at_recv, rs_send, rs_recv,
):
    sp = lax.axis_index("sp")
    tp = lax.axis_index("tp")
    z = sp // NX
    x = sp % NX
    y = tp // 2
    c = tp % 2
    other = 1 - c

    def up_y(d):
        return lax.rem(y + d, NY)

    partner = (sp, y * 2 + other)
    y_next = (sp, up_y(1) * 2 + c)
    y_prev = (sp, up_y(3) * 2 + c)
    x_peer = [None] + [(z * NX + lax.rem(x + d, NX), tp) for d in (1, 2, 3)]
    z_next = (lax.rem(z + 1, NZ) * NX + x, tp)
    z_prev = (lax.rem(z + NZ - 1, NZ) * NX + x, tp)
    s_next = (lax.rem(sp + 1, NZ * NX), tp)
    s_prev = (lax.rem(sp + NZ * NX - 1, NZ * NX), tp)

    def remote(src, dst, ssem, rsem, dev):
        return pltpu.make_async_remote_copy(
            src_ref=src, dst_ref=dst, send_sem=ssem, recv_sem=rsem, device_id=dev, device_id_type=MESH
        )

    load_x = pltpu.make_async_copy(x_hbm, xbuf.at[tp], loc_sem.at[0])
    load_x.start()
    loads = [
        pltpu.make_async_copy(wq_hbm, w.at[0], loc_sem.at[1]),
        pltpu.make_async_copy(wk_hbm, w.at[1], loc_sem.at[2]),
        pltpu.make_async_copy(wv_hbm, w.at[2], loc_sem.at[3]),
        pltpu.make_async_copy(near_hbm, near, loc_sem.at[4]),
        pltpu.make_async_copy(far_hbm, far, loc_sem.at[5]),
    ]
    for copy in loads:
        copy.start()
    load_wo = pltpu.make_async_copy(wo_hbm, wo.at[c], loc_sem.at[6])
    load_wo.start()
    barrier = pltpu.get_barrier_semaphore()
    for dev in [partner, y_next, y_prev, *x_peer[1:], z_next, z_prev, s_next, s_prev]:
        pl.semaphore_signal(barrier, inc=1, device_id=dev, device_id_type=MESH)
    pl.semaphore_wait(barrier, 10)

    top, low = pl.ds(0, SHARD // 2), pl.ds(SHARD // 2, SHARD // 2)

    def shard_copy(i, owner, part, dev):
        return remote(xbuf.at[owner, part], xbuf.at[owner, part], ag_send.at[i], ag_recv.at[i], dev)

    own = y * 2 + c
    below = up_y(3) * 2 + c
    above = up_y(1) * 2 + c
    far_y = up_y(2) * 2 + c
    load_x.wait()
    ag = [
        shard_copy(0, own, top, y_next),
        shard_copy(1, own, low, y_next),
        shard_copy(2, own, top, y_prev),
        shard_copy(3, own, low, y_prev),
        shard_copy(4, below, top, y_next),
        shard_copy(5, above, low, y_prev),
    ]

    def to_partner(i, owner):
        return remote(xbuf.at[owner], xbuf.at[owner], dd_send.at[i], dd_recv.at[i], partner)

    dd = [to_partner(0, own), to_partner(1, below), to_partner(2, above), to_partner(3, far_y)]

    dd[0].start()
    ag[0].start()
    ag[3].start()
    ag[1].start()
    ag[2].start()

    r1 = iota((128, 256), 0)
    k1 = iota((128, 256), 1)
    bias1[...] = jnp.where(jnp.abs(k1 - SIDE - r1) <= SIDE, 0.0, NEG)
    r8 = iota((128, 384), 0)
    k8 = iota((128, 384), 1)
    q_at = (r8 // 16) * 64 + (r8 % 16) * 4
    k_at = (k8 // 128 - 1) * ROWS + ((k8 % 128) // 16) * 64 + (k8 % 16) * 4
    gap = k_at - q_at
    bias8[...] = jnp.where((jnp.abs(gap) <= SIDE * 8) & (gap % 8 == 0), 0.0, NEG)
    r64 = iota((64, 320), 0)
    k64 = iota((64, 320), 1)
    q_step = ((r64 % 8) // 2) * 8 + (r64 // 16) * 2 + r64 % 2
    k_step = ((k64 % 8) // 2) * 8 + ((k64 % 64) // 16) * 2 + k64 % 2
    group = k64 // 64 - 2
    same = (r64 % 16) // 8 == (k64 % 16) // 8
    near_by = jnp.abs(group * 32 + k_step - q_step) <= SIDE
    inside = (z + group >= 0) & (z + group < NZ)
    bias64[...] = jnp.where(same & near_by & inside, 0.0, NEG)
    pr = iota((128, 128), 0)
    pc = iota((128, 128), 1)
    sort_f = ((pr // 8 == pc % 16) & (pr % 8 == pc // 16)).astype(F32)
    sort_b = sort_f.astype(BF)
    back_f = ((pc // 8 == pr % 16) & (pc % 8 == pr // 16)).astype(F32)
    back_b = back_f.astype(BF)

    for copy in loads:
        copy.wait()
    lanes = head_lanes()
    first_half = iota((1, COLS), 1) % 64 < 32

    def project(yc, slot):
        rows = xbuf[pl.ds(yc * 2, 2)].reshape(2 * SHARD, D)

        for j in range(3):
            acc = jnp.dot(rows, w[j], preferred_element_type=F32)
            if j < 2:
                for i in range(2):
                    part = acc[i * SHARD : (i + 1) * SHARD]
                    at = sp * 8 + yc * 2 + i
                    cos_f, sin_f = far[0, pl.ds(at, 1), :], far[1, pl.ds(at, 1), :]
                    cos = near[0] * cos_f - near[1] * sin_f
                    sin = near[1] * cos_f + near[0] * sin_f
                    cos = jnp.concatenate([cos, cos], axis=1)
                    sin = jnp.concatenate([sin, sin], axis=1)
                    swapped = jnp.where(first_half, pltpu.roll(part, COLS - 32, 1), pltpu.roll(part, 32, 1))
                    part = part * cos + swapped * sin
                    if j == 0:
                        part = part * 0.125
                    for n in range(2):
                        rot[j * 2 + n, pl.ds(i * SHARD, SHARD), :] = part[:, n * 128 : (n + 1) * 128]
            else:
                for n in range(2):
                    rot[j * 2 + n] = acc[:, n * 128 : (n + 1) * 128]
        here = pl.multiple_of(yc * 128, 128)
        for n in range(2):
            qn[pl.ds(here, 128), n * 128 : (n + 1) * 128] = rot[n].astype(BF)
        for n in range(4):
            kvn[pl.ds(SHARD + here, 128), n * 128 : (n + 1) * 128] = rot[2 + n].astype(BF)
        for d in range(4):
            residue = lax.rem(x + d, NX)
            picked = [rot[n, pl.ds(residue, 32, stride=4), :].astype(BF) for n in range(6)]
            for n in range(6):
                if d == 0:
                    row = pl.multiple_of(x * 32, 32)
                    if n < 2:
                        qa[yc, pl.ds(row, 32), n * 128 : (n + 1) * 128] = picked[n]
                    else:
                        kv5[2, yc, pl.ds(row, 32), (n - 2) * 128 : (n - 1) * 128] = picked[n]
                elif n < 2:
                    send_q[slot, d - 1, :, n * 128 : (n + 1) * 128] = picked[n]
                else:
                    send_kv[slot, d - 1, :, (n - 2) * 128 : (n - 1) * 128] = picked[n]
        for copy in x_copies(yc, slot):
            copy.start()

    def x_copies(yc, slot):
        mine = pl.ds(pl.multiple_of(x * 32, 32), 32)
        out = []
        for d in (1, 2, 3):
            out.append(
                remote(
                    send_kv.at[slot, d - 1], kv5.at[2, yc, mine],
                    xs_send.at[slot, d - 1, 0], xs_recv.at[slot, d - 1, 0], x_peer[d],
                )
            )
            out.append(
                remote(
                    send_q.at[slot, d - 1], qa.at[yc, mine],
                    xs_send.at[slot, d - 1, 1], xs_recv.at[slot, d - 1, 1], x_peer[d],
                )
            )
        return out

    def wait_x(yc, slot):
        for copy in x_copies(yc, slot):
            copy.wait_recv()

    def z_copies(yc, slot):
        return [
            remote(kv5.at[2, yc], kv5.at[1, yc], z_send.at[slot, 0], z_recv.at[slot, 0], z_next),
            remote(kv5.at[2, yc], kv5.at[3, yc], z_send.at[slot, 1], z_recv.at[slot, 1], z_prev),
            remote(kv5.at[1, yc], kv5.at[0, yc], z_send.at[slot, 2], z_recv.at[slot, 2], z_next),
            remote(kv5.at[3, yc], kv5.at[4, yc], z_send.at[slot, 3], z_recv.at[slot, 3], z_prev),
        ]

    def sort_group(zz, yc):
        kvb[zz * 4 + yc] = jnp.dot(sort_b, kv5[zz, yc], preferred_element_type=F32).astype(BF)

    def z_start(yc, slot):
        copies = z_copies(yc, slot)
        copies[0].start()
        copies[1].start()
        qb[yc] = jnp.dot(sort_b, qa[yc], preferred_element_type=F32).astype(BF)
        sort_group(2, yc)

    def z_forward(yc, slot):
        copies = z_copies(yc, slot)
        copies[0].wait_recv()
        copies[2].start()
        copies[1].wait_recv()
        copies[3].start()
        sort_group(1, yc)
        sort_group(3, yc)

    def z_finish(yc, slot):
        copies = z_copies(yc, slot)
        copies[2].wait_recv()
        sort_group(0, yc)
        copies[3].wait_recv()
        sort_group(4, yc)

    order = [y, up_y(3), up_y(1), up_y(2)]

    dd[0].wait_recv()
    project(order[0], 0)
    ag[0].wait_recv()
    ag[4].start()
    ag[3].wait_recv()
    ag[5].start()
    share_wo = remote(wo_hbm, wo.at[c], wo_send, wo_recv, partner)
    share_wo.start()
    wait_x(order[0], 0)
    z_start(order[0], 0)
    ag[1].wait_recv()
    dd[1].start()
    ag[2].wait_recv()
    dd[2].start()
    z_forward(order[0], 0)
    dd[1].wait_recv()
    project(order[1], 1)
    dd[2].wait_recv()
    project(order[2], 2)
    wait_x(order[1], 1)
    z_start(order[1], 1)
    ag[4].wait_recv()
    ag[5].wait_recv()
    dd[3].start()
    wait_x(order[2], 2)
    z_start(order[2], 2)
    dd[3].wait_recv()
    project(order[3], 3)
    halo = [
        remote(kvn.at[pl.ds(ROWS, SHARD)], kvn.at[pl.ds(0, SHARD)], n_send.at[0], n_recv.at[0], s_next),
        remote(kvn.at[pl.ds(SHARD, SHARD)], kvn.at[pl.ds(ROWS + SHARD, SHARD)], n_send.at[1], n_recv.at[1], s_prev),
    ]
    halo[0].start()
    halo[1].start()
    z_forward(order[1], 1)
    wait_x(order[3], 3)
    z_start(order[3], 3)
    z_forward(order[2], 2)
    z_finish(order[0], 0)

    halo[0].wait_recv()
    halo[1].wait_recv()
    key_at = iota((1, 256), 1)

    def block1(i, carry):
        at = pl.multiple_of(i * 128, 128)
        q = qn[pl.ds(at, 128), :]
        k = kvn[pl.ds(at, 256), 0:COLS]
        v = kvn[pl.ds(at, 256), COLS : 2 * COLS]
        token = sp * ROWS + i * 128 - SIDE + key_at
        edge = jnp.where((token >= 0) & (token < TOKENS), 0.0, NEG)
        out, sums = attend(q, k, v, bias1[...] + edge)
        o1[pl.ds(at, 128), :] = out
        l1[pl.ds(at, 128), :] = sums
        return carry

    lax.fori_loop(0, 4, block1, 0)
    z_forward(order[3], 3)

    section = iota((1, 384), 1) // 128 - 1

    def block8(i, carry):
        q = qa[:, pl.ds(pl.multiple_of(i * 32, 32), 32), :].reshape(128, COLS)
        parts = []
        for step in (-1, 0, 1):
            at = 8 + i + step
            rows = pl.ds(pl.multiple_of(lax.rem(at, 4) * 32, 32), 32)
            parts.append(kv5[lax.div(at, 4), :, rows, :].reshape(128, 2 * COLS))
        kv = jnp.concatenate(parts, axis=0)
        place = z * NX + i + section
        edge = jnp.where((place >= 0) & (place < NZ * NX), 0.0, NEG)
        out, sums = attend(q, kv[:, 0:COLS], kv[:, COLS:], bias8[...] + edge)
        rows = pl.ds(pl.multiple_of(i * 32, 32), 32)
        o8[:, rows, :] = out.reshape(4, 32, COLS)
        l8[:, rows, :] = sums.reshape(4, 32, 128)
        return carry

    lax.fori_loop(0, 4, block8, 0)
    z_finish(order[1], 1)
    z_finish(order[2], 2)
    z_finish(order[3], 3)

    def block64(i, carry):
        rows = pl.ds(pl.multiple_of(i * 16, 16), 16)
        q = qb[:, rows, :].reshape(64, COLS)
        kv = kvb[:, rows, :].reshape(320, 2 * COLS)
        out, sums = attend(q, kv[:, 0:COLS], kv[:, COLS:], bias64[...])
        ob[:, rows, :] = out.astype(BF).reshape(4, 16, COLS)
        lb[:, rows, :] = sums.reshape(4, 16, 128)
        return carry

    lax.fori_loop(0, 8, block64, 0)

    def join(i, carry):
        out64 = jnp.dot(back_b, ob[i], preferred_element_type=F32)
        lse64 = jnp.dot(back_f, lb[i], preferred_element_type=F32, precision=lax.Precision.HIGHEST)
        out, sums = merge(o8[i], l8[i], out64, lse64)
        rows = pl.ds(pl.multiple_of(i * 32, 32), 32)
        ro[:, rows, :] = out.astype(BF).reshape(4, 32, COLS)
        rl[:, rows, :] = sums.reshape(4, 32, 128)
        return carry

    lax.fori_loop(0, 4, join, 0)
    for i in range(4):
        rlt[i] = rl[i].T[0:8, :]
    backs = []
    for d in (1, 2, 3):
        to = lax.rem(x + d, NX)
        backs.append(remote(ro.at[to], ri.at[x], ret_send.at[d - 1, 0], ret_recv.at[d - 1, 0], x_peer[d]))
        backs.append(remote(rlt.at[to], rit.at[x], ret_send.at[d - 1, 1], ret_recv.at[d - 1, 1], x_peer[d]))
    for copy in backs:
        copy.start()
    ri[x] = ro[x]
    rit[x] = rlt[x]
    for copy in backs:
        copy.wait_recv()
    for i in range(4):
        o = ri[i].astype(F32)
        for n in range(2):
            o2[n, pl.ds(i, 128, stride=4), :] = o[:, n * 128 : (n + 1) * 128]
        square = jnp.concatenate([rit[i], jnp.zeros((120, 128), F32)], axis=0).T
        l2[pl.ds(i, 128, stride=4), :] = square

    def last(i, carry):
        rows = pl.ds(pl.multiple_of(i * 128, 128), 128)
        wide = jnp.concatenate([o2[0, rows, :], o2[1, rows, :]], axis=1)
        out, sums = merge(o1[rows, :], l1[rows, :], wide, l2[rows, :])
        att[c, pl.ds(i * 2, 2)] = out.astype(BF).reshape(2, SHARD, COLS)
        logw_ref[i] = sums.T[0:8, :]
        return carry

    lax.fori_loop(0, 4, last, 0)

    trade = []
    for k in range(4):
        u = up_y(k) * 2 + other
        trade.append(remote(att.at[c, u], att.at[c, u], at_send.at[k], at_recv.at[k], partner))
    for copy in trade:
        copy.start()
    load_wo.wait()
    share_wo.wait_recv()
    for copy in trade:
        copy.wait_recv()
    lhs = [
        jnp.concatenate([att[i, up_y(k) * 2 + c] for k in range(4)], axis=0) for i in range(2)
    ]

    def columns(n, carry):
        cols = pl.ds(pl.multiple_of(n * 256, 256), 256)
        acc = jnp.dot(lhs[0], wo[0, :, cols], preferred_element_type=F32)
        acc = acc + jnp.dot(lhs[1], wo[1, :, cols], preferred_element_type=F32)
        inner = pl.ds(pl.multiple_of(lax.rem(n, 8) * 256, 256), 256)
        rb[:, lax.div(n, 8), :, inner] = acc.astype(BF).reshape(4, SHARD, 256)
        return carry

    rs = [
        remote(rb.at[2, 0], rv.at[0], rs_send.at[0], rs_recv.at[0], y_next),
        remote(rb.at[2, 1], rv.at[1], rs_send.at[1], rs_recv.at[1], y_prev),
        remote(rb.at[1, 1], rv.at[2], rs_send.at[2], rs_recv.at[2], y_next),
        remote(rb.at[3, 0], rv.at[3], rs_send.at[3], rs_recv.at[3], y_prev),
        remote(rb.at[1, 0], rv.at[4], rs_send.at[4], rs_recv.at[4], y_next),
        remote(rb.at[3, 1], rv.at[5], rs_send.at[5], rs_recv.at[5], y_prev),
    ]
    lax.fori_loop(0, 8, columns, 0)
    rs[0].start()
    rs[3].start()
    lax.fori_loop(8, 16, columns, 0)
    rs[1].start()
    rs[2].start()

    def add_to(dst, src):
        def step(n, carry):
            cols = pl.ds(pl.multiple_of(n * 512, 512), 512)
            dst[:, cols] = (dst[:, cols].astype(F32) + src[:, cols].astype(F32)).astype(BF)
            return carry

        lax.fori_loop(0, 4, step, 0)

    rs[0].wait_recv()
    add_to(rb.at[1, 0], rv.at[0])
    rs[4].start()
    rs[1].wait_recv()
    add_to(rb.at[3, 1], rv.at[1])
    rs[5].start()
    for i in (2, 3, 4, 5):
        rs[i].wait_recv()
    for half, pair in ((0, (3, 4)), (1, (2, 5))):
        def total(n, carry, half=half, pair=pair):
            cols = pl.ds(pl.multiple_of(n * 512, 512), 512)
            acc = rb[0, half, :, cols].astype(F32) + rv[pair[0], :, cols].astype(F32)
            acc = acc + rv[pair[1], :, cols].astype(F32)
            mixed_ref[:, pl.ds(pl.multiple_of(half * HALF + n * 512, 512), 512)] = acc.astype(BF)
            return carry

        lax.fori_loop(0, 4, total, 0)

    for copy in ag + dd + [share_wo] + halo + backs + trade + rs:
        copy.wait_send()
    for slot in range(4):
        for copy in x_copies(order[slot], slot) + z_copies(order[slot], slot):
            copy.wait_send()


def per_device(tokens_in, w_query, w_key, w_value, w_out):
    near, far = rotary_tables()
    dma = pltpu.SemaphoreType.DMA
    vm = pltpu.VMEM
    scratch = [
        vm((8, SHARD, D), BF),
        vm((3, D, COLS), BF),
        vm((2, COLS, D), BF),
        vm((2, SHARD, 128), F32),
        vm((2, TOKENS // SHARD, 128), F32),
        vm((6, 128, 128), F32),
        vm((ROWS, COLS), BF),
        vm((ROWS + 2 * SHARD, 2 * COLS), BF),
        vm((4, 3, 32, COLS), BF),
        vm((4, 3, 32, 2 * COLS), BF),
        vm((4, 128, COLS), BF),
        vm((5, 4, 128, 2 * COLS), BF),
        vm((4, 128, COLS), BF),
        vm((20, 128, 2 * COLS), BF),
        vm((128, 256), F32),
        vm((128, 384), F32),
        vm((64, 320), F32),
        vm((4, 128, COLS), F32),
        vm((4, 128, 128), F32),
        vm((4, 128, COLS), BF),
        vm((4, 128, 128), F32),
        vm((4, 128, COLS), BF),
        vm((4, 128, 128), F32),
        vm((4, 8, 128), F32),
        vm((4, 128, COLS), BF),
        vm((4, 8, 128), F32),
        vm((ROWS, COLS), F32),
        vm((ROWS, 128), F32),
        vm((2, ROWS, 128), F32),
        vm((ROWS, 128), F32),
        vm((2, 8, SHARD, COLS), BF),
        vm((4, 2, SHARD, HALF), BF),
        vm((6, SHARD, HALF), BF),
        dma((7,)),
        dma((6,)), dma((6,)),
        dma((4,)), dma((4,)),
        dma(()), dma(()),
        dma((4, 3, 2)), dma((4, 3, 2)),
        dma((4, 4)), dma((4, 4)),
        dma((2,)), dma((2,)),
        dma((3, 2)), dma((3, 2)),
        dma((4,)), dma((4,)),
        dma((6,)), dma((6,)),
    ]
    hbm = pl.BlockSpec(memory_space=pl.ANY)
    vmem = pl.BlockSpec(memory_space=pltpu.VMEM)
    mixed, logw = pl.pallas_call(
        kernel,
        out_shape=(jax.ShapeDtypeStruct((SHARD, D), BF), jax.ShapeDtypeStruct((4, 8, 128), F32)),
        in_specs=[hbm] * 7,
        out_specs=(vmem, vmem),
        scratch_shapes=scratch,
        compiler_params=pltpu.CompilerParams(
            collective_id=0, has_side_effects=True, vmem_limit_bytes=60 * 1024 * 1024
        ),
    )(tokens_in, w_query, w_key, w_value, w_out, jnp.asarray(near), jnp.asarray(far))
    log_weight = jnp.transpose(logw[:, 0:4, :], (1, 0, 2)).reshape(4, ROWS)
    return mixed, log_weight


def solution(mesh):
    in_specs = (P(("sp", "tp"), None), P(None, "tp"), P(None, "tp"), P(None, "tp"), P("tp", None))
    out_specs = (P(("sp", "tp"), None), P("tp", "sp"))
    return jax.shard_map(per_device, mesh=mesh, in_specs=in_specs, out_specs=out_specs, check_vma=False)
```

profile of v0, /device:TPU:1, one launch (start us, length us, event | category | flops | bytes accessed | tf_op | source)
XLA Modules:
  0.0 93.4 jit_solution(4545760760557107214)
XLA Ops:
  0.6 89.6 %shard_map.86 = (bf16[64,4096]{1,0:T(8,128)(2,1)}, f32[4,8,128]{2,1,0:T(8,128)}) custom-call(bf16[64,4096]{1,0:T(8,128)(2,1)} %x_hbm.1, bf16[4096,256]{1,0:T(8,128)(2,1)} %wq_hbm.1, bf16[4096,256]{1,0:T(8,128)(2,1)} %wk_hbm.1, bf16[4096,256]{1,0:T(8,128)(2,1)} %wv_hbm.1, bf16[256,4096]{1,0:T(8,128)(2,1)} %wo_hbm.1, f32[2,64,128]{2,1,0:T(8,128)} %constant.4.clone.near_hbm, ...), custom_call_target="tpu_custom_call" | custom-call | tf_op jit(solution)/shard_map/pallas_call | solution.py:555
  90.2 1.3 %slice_bitcast_fusion = f32[4,512]{1,0:T(4,128)} fusion(f32[4,8,128]{2,1,0:T(8,128)} %get-tuple-element.5), kind=kLoop, calls=%fused_computation | loop fusion | bytes 16384 | tf_op jit(solution)/shard_map/reshape | solution.py:565
  91.5 1.9 %copy.10 = bf16[64,4096]{1,0:T(8,128)(2,1)} copy(bf16[64,4096]{1,0:T(8,128)(2,1)} %get-tuple-element.8) | data formatting | bytes 1048576
where the time goes:
time: 93.6 us; the launch traced here: 93.4 us
  Pallas kernels  89.6 us (96%)
  local copies, waits for them, and re-layouts  3.19 us (3%)
    pallas_call x1, Pallas kernels, per_device(): pl.pallas_call(kernel, out_shape=(jax.ShapeDtypeStruct((SHARD, D), BF), j...  89.6 us

commit v1 on v0

v1 whole, which is shorter than its diff:
```python
import functools

import jax
import jax.numpy as jnp
import numpy as np
from jax import lax
from jax.experimental import pallas as pl
from jax.experimental.pallas import tpu as pltpu
from jax.sharding import PartitionSpec as P

NZ, NX, NY = 8, 4, 4
SHARD = 64
ROWS = 512
D = 4096
COLS = 256
SIDE = 64
TOKENS = 16384
ROTARY_BASE = 500000.0
NEG = -1e30
MESH = pl.DeviceIdType.MESH
BF = jnp.bfloat16
F32 = jnp.float32
NT = (((1,), (1,)), ((), ()))


def rotary_tables():
    lane = np.arange(128)
    freq = ROTARY_BASE ** (-(lane % 32) / 32.0)
    sign = np.where(lane % 64 < 32, -1.0, 1.0)
    near = np.arange(SHARD)[:, None] * freq[None, :]
    far = (np.arange(TOKENS // SHARD) * SHARD)[:, None] * freq[None, :]
    near = np.stack([np.cos(near), sign * np.sin(near)])
    far = np.stack([np.cos(far), sign * np.sin(far)])
    return near.astype(np.float32), far.astype(np.float32)


def iota(shape, dim):
    return lax.broadcasted_iota(jnp.int32, shape, dim)


def head_lanes(width=COLS):
    return iota((1, width), 1) // 64


def attend(q, k, v, bias):
    rows = q.shape[0]
    lanes = head_lanes()
    stacked = jnp.concatenate([q * (lanes == h).astype(F32).astype(BF) for h in range(4)], axis=0)
    scores = lax.dot_general(stacked, k, NT, preferred_element_type=F32)
    scores = scores + jnp.concatenate([bias] * 4, axis=0)
    top = jnp.max(scores, axis=1, keepdims=True)
    expo = jnp.exp(scores - top)
    total = jnp.sum(expo, axis=1, keepdims=True)
    out = jnp.dot(expo.astype(BF), v, preferred_element_type=F32) / total
    lse = top + jnp.log(total)
    small = iota((1, 128), 1)
    merged = jnp.zeros((rows, COLS), F32)
    sums = jnp.zeros((rows, 128), F32)
    for h in range(4):
        part = slice(h * rows, (h + 1) * rows)
        merged = jnp.where(lanes == h, out[part], merged)
        sums = jnp.where(small == h, lse[part], sums)
    return merged, sums


def merge(out_a, lse_a, out_b, lse_b):
    peak = jnp.maximum(lse_a, lse_b)
    share_a = jnp.exp(lse_a - peak)
    share_b = jnp.exp(lse_b - peak)
    total = share_a + share_b
    lanes = head_lanes()
    wide_a = jnp.zeros(out_a.shape, F32)
    wide_b = jnp.zeros(out_a.shape, F32)
    share_a = share_a / total
    share_b = share_b / total
    for h in range(4):
        wide_a = jnp.where(lanes == h, share_a[:, h : h + 1], wide_a)
        wide_b = jnp.where(lanes == h, share_b[:, h : h + 1], wide_b)
    return wide_a * out_a + wide_b * out_b, peak + jnp.log(total)


def kernel(
    x_hbm, wq_hbm, wk_hbm, wv_hbm, wo_hbm, near_hbm, far_hbm,
    mixed_ref, logw_ref,
    xbuf, w, wo, near, far,
    rot, qn, kvn, send_q, send_kv, qa, kv5, qb, kvb,
    bias1, bias8, bias64,
    o8, l8, ob, lb, ro, rl, rlt, ri, rit, o1, l1, o2, l2,
    att, rb, rv,
    loc_sem, ag_send, ag_recv, dd_send, dd_recv, wo_send, wo_recv,
    xs_send, xs_recv, xq_send, xq_recv, z_send, z_recv, n_send, n_recv, ret_send, ret_recv,
    at_send, at_recv, rs_send, rs_recv,
):
    sp = lax.axis_index("sp")
    tp = lax.axis_index("tp")
    z = sp // NX
    x = sp % NX
    y = tp // 2
    c = tp % 2
    other = 1 - c

    def up_y(d):
        return lax.rem(y + d, NY)

    partner = (sp, y * 2 + other)
    y_next = (sp, up_y(1) * 2 + c)
    y_prev = (sp, up_y(3) * 2 + c)
    x_peer = [None] + [(z * NX + lax.rem(x + d, NX), tp) for d in (1, 2, 3)]
    z_next = (lax.rem(z + 1, NZ) * NX + x, tp)
    z_prev = (lax.rem(z + NZ - 1, NZ) * NX + x, tp)
    s_next = (lax.rem(sp + 1, NZ * NX), tp)
    s_prev = (lax.rem(sp + NZ * NX - 1, NZ * NX), tp)

    def remote(src, dst, ssem, rsem, dev):
        return pltpu.make_async_remote_copy(
            src_ref=src, dst_ref=dst, send_sem=ssem, recv_sem=rsem, device_id=dev, device_id_type=MESH
        )

    load_x = pltpu.make_async_copy(x_hbm, xbuf.at[tp], loc_sem.at[0])
    load_x.start()
    loads = [
        pltpu.make_async_copy(wq_hbm, w.at[0], loc_sem.at[1]),
        pltpu.make_async_copy(wk_hbm, w.at[1], loc_sem.at[2]),
        pltpu.make_async_copy(wv_hbm, w.at[2], loc_sem.at[3]),
        pltpu.make_async_copy(near_hbm, near, loc_sem.at[4]),
        pltpu.make_async_copy(far_hbm, far, loc_sem.at[5]),
    ]
    for copy in loads:
        copy.start()
    load_wo = pltpu.make_async_copy(wo_hbm, wo.at[c], loc_sem.at[6])
    load_wo.start()
    barrier = pltpu.get_barrier_semaphore()
    for dev in [partner, y_next, y_prev, *x_peer[1:], z_next, z_prev, s_next, s_prev]:
        pl.semaphore_signal(barrier, inc=1, device_id=dev, device_id_type=MESH)
    pl.semaphore_wait(barrier, 10)

    top, low = pl.ds(0, SHARD // 2), pl.ds(SHARD // 2, SHARD // 2)

    def shard_copy(i, owner, part, dev):
        return remote(xbuf.at[owner, part], xbuf.at[owner, part], ag_send.at[i], ag_recv.at[i], dev)

    own = y * 2 + c
    below = up_y(3) * 2 + c
    above = up_y(1) * 2 + c
    far_y = up_y(2) * 2 + c
    load_x.wait()
    ag = [
        shard_copy(0, own, top, y_next),
        shard_copy(1, own, low, y_next),
        shard_copy(2, own, top, y_prev),
        shard_copy(3, own, low, y_prev),
        shard_copy(4, below, top, y_next),
        shard_copy(5, above, low, y_prev),
    ]

    def to_partner(i, owner, part=None):
        ref = xbuf.at[owner] if part is None else xbuf.at[owner, part]
        return remote(ref, ref, dd_send.at[i], dd_recv.at[i], partner)

    dd = [
        to_partner(0, own),
        to_partner(1, below, top),
        to_partner(2, above, low),
        to_partner(3, below, low),
        to_partner(4, above, top),
        to_partner(5, far_y, top),
        to_partner(6, far_y, low),
    ]

    dd[0].start()
    ag[0].start()
    ag[3].start()
    ag[1].start()
    ag[2].start()

    r1 = iota((128, 256), 0)
    k1 = iota((128, 256), 1)
    bias1[...] = jnp.where(jnp.abs(k1 - SIDE - r1) <= SIDE, 0.0, NEG)
    r8 = iota((128, 384), 0)
    k8 = iota((128, 384), 1)

    def token8(r):
        return (r // 32) * 128 + ((r % 32) // 16) * 32 + ((r % 16) // 8) * 64 + (r % 8) * 4

    gap = (k8 // 128 - 1) * ROWS + token8(k8 % 128) - token8(r8)
    bias8[...] = jnp.where((jnp.abs(gap) <= SIDE * 8) & (gap % 8 == 0), 0.0, NEG)
    r64 = iota((64, 320), 0)
    k64 = iota((64, 320), 1)
    q_step = ((r64 % 8) // 2) * 8 + (r64 // 16) * 2 + r64 % 2
    k_step = ((k64 % 8) // 2) * 8 + ((k64 % 64) // 16) * 2 + k64 % 2
    group = k64 // 64 - 2
    same = (r64 % 16) // 8 == (k64 % 16) // 8
    near_by = jnp.abs(group * 32 + k_step - q_step) <= SIDE
    inside = (z + group >= 0) & (z + group < NZ)
    bias64[...] = jnp.where(same & near_by & inside, 0.0, NEG)
    pr = iota((128, 128), 0)
    pc = iota((128, 128), 1)
    swap = (pr // 64 == pc // 64) & ((pr % 64) // 8 == pc % 8) & (pr % 8 == (pc % 64) // 8)
    swap_f = swap.astype(F32)
    swap_b = swap_f.astype(BF)
    swap_half = swap_b[0:64, 0:64]

    for copy in loads:
        copy.wait()
    lanes = head_lanes()
    first_half = iota((1, COLS), 1) % 64 < 32

    slots = [
        [(y, 0), (y, 1)],
        [(up_y(3), 0), (up_y(1), 1)],
        [(up_y(3), 1), (up_y(1), 0)],
        [(up_y(2), 0), (up_y(2), 1)],
    ]

    def project(slot):
        pieces = [(yc, half, i) for yc, half in slots[slot] for i in range(2)]
        rows = jnp.concatenate(
            [xbuf[yc * 2 + i, half * 32 : half * 32 + 32, :] for yc, half, i in pieces], axis=0
        )
        for j in (1, 2, 0):
            acc = jnp.dot(rows, w[j], preferred_element_type=F32)
            if j < 2:
                for m, (yc, half, i) in enumerate(pieces):
                    part = acc[m * 32 : (m + 1) * 32]
                    at = sp * 8 + yc * 2 + i
                    cos_f, sin_f = far[0, pl.ds(at, 1), :], far[1, pl.ds(at, 1), :]
                    cos_n = near[0, half * 32 : half * 32 + 32, :]
                    sin_n = near[1, half * 32 : half * 32 + 32, :]
                    cos = cos_n * cos_f - sin_n * sin_f
                    sin = sin_n * cos_f + cos_n * sin_f
                    cos = jnp.concatenate([cos, cos], axis=1)
                    sin = jnp.concatenate([sin, sin], axis=1)
                    swapped = jnp.where(first_half, pltpu.roll(part, COLS - 32, 1), pltpu.roll(part, 32, 1))
                    part = part * cos + swapped * sin
                    if j == 0:
                        part = part * 0.125
                    for n in range(2):
                        rot[j * 2 + n, m * 32 : (m + 1) * 32, :] = part[:, n * 128 : (n + 1) * 128]
            else:
                for n in range(2):
                    rot[j * 2 + n] = acc[:, n * 128 : (n + 1) * 128]
            for d in range(4):
                residue = lax.rem(x + d, NX)
                for e, (yc, half) in enumerate(slots[slot]):
                    row = pl.multiple_of(x * 16, 16)
                    for n in range(2):
                        picked = rot[j * 2 + n, pl.ds(e * 64 + residue, 16, stride=4), :].astype(BF)
                        cols = slice(n * 128, (n + 1) * 128)
                        wide = slice((j - 1) * COLS + n * 128, (j - 1) * COLS + (n + 1) * 128)
                        if d == 0 and j == 0:
                            qa[yc * 2 + half, pl.ds(row, 16), cols] = picked
                        elif d == 0:
                            kv5[2, yc * 2 + half, pl.ds(row, 16), wide] = picked
                        elif j == 0:
                            send_q[slot, d - 1, e, :, cols] = picked
                        else:
                            send_kv[slot, d - 1, e, :, wide] = picked
            if j == 2:
                for copy in kv_copies(slot):
                    copy.start()
        for copy in q_copies(slot):
            copy.start()
        for m, (yc, half, i) in enumerate(pieces):
            here = pl.multiple_of(yc * 128 + i * 64 + half * 32, 32)
            part = slice(m * 32, (m + 1) * 32)
            for n in range(2):
                qn[pl.ds(here, 32), n * 128 : (n + 1) * 128] = rot[n, part, :].astype(BF)
            for n in range(4):
                kvn[pl.ds(SIDE + here, 32), n * 128 : (n + 1) * 128] = rot[2 + n, part, :].astype(BF)

    mine = pl.ds(pl.multiple_of(x * 16, 16), 16)

    def kv_copies(slot):
        return [
            remote(
                send_kv.at[slot, d - 1, e], kv5.at[2, yc * 2 + half, mine],
                xs_send.at[slot, d - 1, e], xs_recv.at[slot, d - 1, e], x_peer[d],
            )
            for d in (2, 1, 3)
            for e, (yc, half) in enumerate(slots[slot])
        ]

    def q_copies(slot):
        return [
            remote(
                send_q.at[slot, d - 1, e], qa.at[yc * 2 + half, mine],
                xq_send.at[slot, d - 1, e], xq_recv.at[slot, d - 1, e], x_peer[d],
            )
            for d in (2, 1, 3)
            for e, (yc, half) in enumerate(slots[slot])
        ]

    def z_copies(slot):
        out = []
        for e, (yc, half) in enumerate(slots[slot]):
            hc = yc * 2 + half
            route = [(2, 1, z_next), (2, 3, z_prev), (1, 0, z_next), (3, 4, z_prev)]
            out.append(
                [
                    remote(kv5.at[a, hc], kv5.at[b, hc], z_send.at[slot, e, i], z_recv.at[slot, e, i], dev)
                    for i, (a, b, dev) in enumerate(route)
                ]
            )
        return out

    def sort_half(zz, yc, half):
        kvb[zz * 4 + yc, half] = jnp.dot(swap_half, kv5[zz, yc * 2 + half], preferred_element_type=F32).astype(BF)

    def z_start(slot):
        for copy in kv_copies(slot):
            copy.wait_recv()
        for copies in z_copies(slot):
            copies[0].start()
            copies[1].start()
        for yc, half in slots[slot]:
            sort_half(2, yc, half)

    def z_forward(slot):
        for copies in z_copies(slot):
            copies[0].wait_recv()
            copies[2].start()
            copies[1].wait_recv()
            copies[3].start()
        for yc, half in slots[slot]:
            sort_half(1, yc, half)
            sort_half(3, yc, half)

    def z_finish(slot):
        for copies in z_copies(slot):
            copies[2].wait_recv()
            copies[3].wait_recv()
        for yc, half in slots[slot]:
            sort_half(0, yc, half)
            sort_half(4, yc, half)

    def q_finish(slot):
        for copy in q_copies(slot):
            copy.wait_recv()
        for yc, half in slots[slot]:
            qb[yc, half] = jnp.dot(swap_half, qa[yc * 2 + half], preferred_element_type=F32).astype(BF)

    key_at = iota((1, 256), 1)

    def block1(i):
        at = pl.multiple_of(i * 128, 128)
        q = qn[pl.ds(at, 128), :]
        k = kvn[pl.ds(at, 256), 0:COLS]
        v = kvn[pl.ds(at, 256), COLS : 2 * COLS]
        token = sp * ROWS + i * 128 - SIDE + key_at
        edge = jnp.where((token >= 0) & (token < TOKENS), 0.0, NEG)
        out, sums = attend(q, k, v, bias1[...] + edge)
        o1[pl.ds(at, 128), :] = out
        l1[pl.ds(at, 128), :] = sums

    dd[0].wait_recv()
    project(0)
    ag[0].wait_recv()
    ag[4].start()
    dd[1].start()
    ag[3].wait_recv()
    ag[5].start()
    dd[2].start()
    z_start(0)
    share_wo = remote(wo_hbm, wo.at[c], wo_send, wo_recv, partner)
    dd[1].wait_recv()
    dd[2].wait_recv()
    project(1)
    z_forward(0)
    ag[1].wait_recv()
    dd[3].start()
    ag[2].wait_recv()
    dd[4].start()
    dd[3].wait_recv()
    dd[4].wait_recv()
    project(2)
    z_start(1)
    ag[4].wait_recv()
    dd[5].start()
    ag[5].wait_recv()
    dd[6].start()
    share_wo.start()
    z_forward(1)
    dd[5].wait_recv()
    dd[6].wait_recv()
    project(3)
    halo = [
        remote(kvn.at[pl.ds(ROWS, SHARD)], kvn.at[pl.ds(0, SHARD)], n_send.at[0], n_recv.at[0], s_next),
        remote(kvn.at[pl.ds(SHARD, SHARD)], kvn.at[pl.ds(ROWS + SHARD, SHARD)], n_send.at[1], n_recv.at[1], s_prev),
    ]
    halo[0].start()
    halo[1].start()
    z_start(2)
    block1(1)
    block1(2)
    z_start(3)
    z_forward(2)
    halo[0].wait_recv()
    halo[1].wait_recv()
    block1(0)
    block1(3)
    for slot in range(4):
        q_finish(slot)
    z_forward(3)

    section = iota((1, 384), 1) // 128 - 1

    def block8(i):
        q = qa[:, pl.ds(pl.multiple_of(i * 16, 16), 16), :].reshape(128, COLS)
        parts = []
        for step in (-1, 0, 1):
            at = 8 + i + step
            rows = pl.ds(pl.multiple_of(lax.rem(at, 4) * 16, 16), 16)
            parts.append(kv5[lax.div(at, 4), :, rows, :].reshape(128, 2 * COLS))
        kv = jnp.concatenate(parts, axis=0)
        place = z * NX + i + section
        edge = jnp.where((place >= 0) & (place < NZ * NX), 0.0, NEG)
        out, sums = attend(q, kv[:, 0:COLS], kv[:, COLS:], bias8[...] + edge)
        rows = pl.ds(pl.multiple_of(i * 16, 16), 16)
        o8[:, rows, :] = out.reshape(8, 16, COLS)
        l8[:, rows, :] = sums.reshape(8, 16, 128)

    def two(block):
        def body(i, carry):
            block(i * 2)
            block(i * 2 + 1)
            return carry

        return body

    lax.fori_loop(0, 2, two(block8), 0)
    for slot in range(4):
        z_finish(slot)

    def block64(i):
        half = lax.div(i, 4)
        rows = pl.ds(pl.multiple_of(lax.rem(i, 4) * 16, 16), 16)
        q = qb[:, half, rows, :].reshape(64, COLS)
        kv = kvb[:, half, rows, :].reshape(320, 2 * COLS)
        out, sums = attend(q, kv[:, 0:COLS], kv[:, COLS:], bias64[...])
        ob[:, half, rows, :] = out.astype(BF).reshape(4, 16, COLS)
        lb[:, half, rows, :] = sums.reshape(4, 16, 128)

    lax.fori_loop(0, 4, two(block64), 0)

    def join(i):
        out64 = jnp.dot(swap_b, ob[i].reshape(128, COLS), preferred_element_type=F32)
        lse64 = jnp.dot(swap_f, lb[i].reshape(128, 128), preferred_element_type=F32, precision=lax.Precision.HIGHEST)
        two_halves = pl.ds(i * 2, 2)
        out, sums = merge(
            o8[two_halves].reshape(128, COLS), l8[two_halves].reshape(128, 128), out64, lse64
        )
        out = out.astype(BF)
        for half in range(2):
            rows = pl.ds(pl.multiple_of(i * 32 + half * 16, 16), 16)
            ro[:, rows, :] = out[half * 64 : half * 64 + 64].reshape(4, 16, COLS)
            rl[:, rows, :] = sums[half * 64 : half * 64 + 64].reshape(4, 16, 128)

    lax.fori_loop(0, 2, two(join), 0)
    for i in range(4):
        rlt[i] = rl[i].T[0:8, :]
    backs = []
    for d in (2, 1, 3):
        to = lax.rem(x + d, NX)
        backs.append(remote(ro.at[to], ri.at[x], ret_send.at[d - 1, 0], ret_recv.at[d - 1, 0], x_peer[d]))
        backs.append(remote(rlt.at[to], rit.at[x], ret_send.at[d - 1, 1], ret_recv.at[d - 1, 1], x_peer[d]))
    for copy in backs:
        copy.start()
    ri[x] = ro[x]
    rit[x] = rlt[x]
    for copy in backs:
        copy.wait_recv()
    for i in range(4):
        o = ri[i].astype(F32)
        square = jnp.concatenate([rit[i], jnp.zeros((120, 128), F32)], axis=0).T
        for m in range(16):
            at = (m // 4) * 128 + (m % 4 // 2) * 32 + (m % 2) * 64 + i
            part = slice(m * 8, m * 8 + 8)
            for n in range(2):
                o2[n, pl.ds(at, 8, stride=4), :] = o[part, n * 128 : (n + 1) * 128]
            l2[pl.ds(at, 8, stride=4), :] = square[part]

    def last(i):
        rows = slice(i * 128, (i + 1) * 128)
        wide = jnp.concatenate([o2[0, rows, :], o2[1, rows, :]], axis=1)
        out, sums = merge(o1[rows, :], l1[rows, :], wide, l2[rows, :])
        att[c, i * 2 : i * 2 + 2] = out.astype(BF).reshape(2, SHARD, COLS)
        logw_ref[:, rows] = sums.T[0:4, :]

    for i in range(4):
        last(i)

    trade = []
    for k in range(4):
        u = up_y(k) * 2 + other
        trade.append(remote(att.at[c, u], att.at[c, u], at_send.at[k], at_recv.at[k], partner))
    for copy in trade:
        copy.start()
    load_wo.wait()
    share_wo.wait_recv()
    for copy in trade:
        copy.wait_recv()
    lhs = [
        jnp.concatenate([att[i, up_y(k) * 2 + c] for k in range(4)], axis=0) for i in range(2)
    ]

    def columns(n):
        cols = slice(n * 512, (n + 1) * 512)
        acc = jnp.dot(lhs[0], wo[0, :, cols], preferred_element_type=F32)
        acc = acc + jnp.dot(lhs[1], wo[1, :, cols], preferred_element_type=F32)
        rb[:, n] = acc.astype(BF).reshape(4, SHARD, 512)

    def rs(i, n, src, dev):
        return remote(rb.at[src, n], rv.at[i, n // 2], rs_send.at[i, n // 2], rs_recv.at[i, n // 2], dev)

    even = range(0, 8, 2)
    odd = range(1, 8, 2)
    first_n = {n: rs(0, n, 2, y_next) for n in even}
    first_p = {n: rs(1, n, 2, y_prev) for n in odd}
    direct_n = {n: rs(2, n, 1, y_next) for n in odd}
    direct_p = {n: rs(3, n, 3, y_prev) for n in even}
    sum_n = {n: rs(4, n, 1, y_next) for n in even}
    sum_p = {n: rs(5, n, 3, y_prev) for n in odd}
    for n in range(8):
        columns(n)
        if n % 2 == 0:
            first_n[n].start()
        else:
            first_p[n].start()
    for n in range(0, 8, 2):
        direct_n[n + 1].start()
        direct_p[n].start()

    for n in range(0, 8, 2):
        first_n[n].wait_recv()
        rb[1, n] = (rb[1, n].astype(F32) + rv[0, n // 2].astype(F32)).astype(BF)
        sum_n[n].start()
        first_p[n + 1].wait_recv()
        rb[3, n + 1] = (rb[3, n + 1].astype(F32) + rv[1, n // 2].astype(F32)).astype(BF)
        sum_p[n + 1].start()
    for n in range(0, 8, 2):
        direct_n[n + 1].wait_recv()
        direct_p[n].wait_recv()
    for n in range(8):
        one, other_one = ((direct_p, sum_n) if n % 2 == 0 else (direct_n, sum_p))
        other_one[n].wait_recv()
        acc = rb[0, n].astype(F32) + rv[3 if n % 2 == 0 else 2, n // 2].astype(F32)
        acc = acc + rv[4 if n % 2 == 0 else 5, n // 2].astype(F32)
        mixed_ref[:, n * 512 : (n + 1) * 512] = acc.astype(BF)

    for copy in ag + dd + [share_wo] + halo + backs + trade:
        copy.wait_send()
    for group in (first_n, first_p, direct_n, direct_p, sum_n, sum_p):
        for copy in group.values():
            copy.wait_send()
    for slot in range(4):
        for copy in kv_copies(slot) + q_copies(slot):
            copy.wait_send()
        for copies in z_copies(slot):
            for copy in copies:
                copy.wait_send()


def per_device(tokens_in, w_query, w_key, w_value, w_out):
    near, far = rotary_tables()
    dma = pltpu.SemaphoreType.DMA
    vm = pltpu.VMEM
    scratch = [
        vm((8, SHARD, D), BF),
        vm((3, D, COLS), BF),
        vm((2, COLS, D), BF),
        vm((2, SHARD, 128), F32),
        vm((2, TOKENS // SHARD, 128), F32),
        vm((6, 128, 128), F32),
        vm((ROWS, COLS), BF),
        vm((ROWS + 2 * SHARD, 2 * COLS), BF),
        vm((4, 3, 2, 16, COLS), BF),
        vm((4, 3, 2, 16, 2 * COLS), BF),
        vm((8, 64, COLS), BF),
        vm((5, 8, 64, 2 * COLS), BF),
        vm((4, 2, 64, COLS), BF),
        vm((20, 2, 64, 2 * COLS), BF),
        vm((128, 256), F32),
        vm((128, 384), F32),
        vm((64, 320), F32),
        vm((8, 64, COLS), F32),
        vm((8, 64, 128), F32),
        vm((4, 2, 64, COLS), BF),
        vm((4, 2, 64, 128), F32),
        vm((4, 128, COLS), BF),
        vm((4, 128, 128), F32),
        vm((4, 8, 128), F32),
        vm((4, 128, COLS), BF),
        vm((4, 8, 128), F32),
        vm((ROWS, COLS), F32),
        vm((ROWS, 128), F32),
        vm((2, ROWS, 128), F32),
        vm((ROWS, 128), F32),
        vm((2, 8, SHARD, COLS), BF),
        vm((4, 8, SHARD, 512), BF),
        vm((6, 4, SHARD, 512), BF),
        dma((7,)),
        dma((6,)), dma((6,)),
        dma((7,)), dma((7,)),
        dma(()), dma(()),
        dma((4, 3, 2)), dma((4, 3, 2)),
        dma((4, 3, 2)), dma((4, 3, 2)),
        dma((4, 2, 4)), dma((4, 2, 4)),
        dma((2,)), dma((2,)),
        dma((3, 2)), dma((3, 2)),
        dma((4,)), dma((4,)),
        dma((6, 4)), dma((6, 4)),
    ]
    hbm = pl.BlockSpec(memory_space=pl.ANY)
    vmem = pl.BlockSpec(memory_space=pltpu.VMEM)
    return pl.pallas_call(
        kernel,
        out_shape=(jax.ShapeDtypeStruct((SHARD, D), BF), jax.ShapeDtypeStruct((4, ROWS), F32)),
        in_specs=[hbm] * 7,
        out_specs=(vmem, vmem),
        scratch_shapes=scratch,
        compiler_params=pltpu.CompilerParams(
            collective_id=0, has_side_effects=True, vmem_limit_bytes=60 * 1024 * 1024
        ),
    )(tokens_in, w_query, w_key, w_value, w_out, jnp.asarray(near), jnp.asarray(far))


def solution(mesh):
    in_specs = (P(("sp", "tp"), None), P(None, "tp"), P(None, "tp"), P(None, "tp"), P("tp", None))
    out_specs = (P(("sp", "tp"), None), P("tp", "sp"))
    return jax.shard_map(per_device, mesh=mesh, in_specs=in_specs, out_specs=out_specs, check_vma=False)
```

time: 93.6 us -> 86.6 us (0.925)
  Pallas kernels: 89.6 us -> 82.7 us
    pallas_call x1, Pallas kernels: 89.6 us -> 82.7 us  [per_device(): pl.pallas_call(kernel, out_shape=(jax.ShapeDtypeStruct((SHARD, D), BF), j...]
    reshape x1 -> x0, local copies, waits for them, and re-layouts: 1.32 us -> none  [per_device(): log_weight = jnp.transpose(logw[:, 0:4, :], (1, 0, 2)).reshape(4, ROWS)]
    unnamed x1 -> x2, local copies, waits for them, and re-layouts: 1.87 us -> 3.16 us
where the time goes in v1:
time: 86.6 us; the launch traced here: 86.5 us
  Pallas kernels  82.7 us (95%)
  local copies, waits for them, and re-layouts  3.16 us (4%)
    pallas_call x1, Pallas kernels, per_device(): pl.pallas_call(kernel, out_shape=(jax.ShapeDtypeStruct((SHARD, D), BF), j...  82.7 us
    unnamed x2, local copies, waits for them, and re-layouts  3.16 us

profile of v1, /device:TPU:1, one launch (start us, length us, event | category | flops | bytes accessed | tf_op | source)
XLA Modules:
  0.0 86.5 jit_solution(7085172090540538479)
XLA Ops:
  0.6 82.7 %shard_map.86 = (bf16[64,4096]{1,0:T(8,128)(2,1)}, f32[4,512]{1,0:T(4,128)}) custom-call(bf16[64,4096]{1,0:T(8,128)(2,1)} %x_hbm.1, bf16[4096,256]{1,0:T(8,128)(2,1)} %wq_hbm.1, bf16[4096,256]{1,0:T(8,128)(2,1)} %wk_hbm.1, bf16[4096,256]{1,0:T(8,128)(2,1)} %wv_hbm.1, bf16[256,4096]{1,0:T(8,128)(2,1)} %wo_hbm.1, f32[2,64,128]{2,1,0:T(8,128)} %constant.4.clone.near_hbm, ...), custom_call_target="tpu_custom_call" | custom-call | tf_op jit(solution)/shard_map/pallas_call | solution.py:615
  83.3 1.9 %copy.11 = bf16[64,4096]{1,0:T(8,128)(2,1)} copy(bf16[64,4096]{1,0:T(8,128)(2,1)} %get-tuple-element.4) | data formatting | bytes 1048576
  85.2 1.3 %copy.12 = f32[4,512]{1,0:T(4,128)} copy(f32[4,512]{1,0:T(4,128)} %get-tuple-element.5) | data formatting | bytes 16384

commit v2 on v1

--- a/solution.py
+++ b/solution.py
@@ -85,7 +85,7 @@
     xbuf, w, wo, near, far,
     rot, qn, kvn, send_q, send_kv, qa, kv5, qb, kvb,
     bias1, bias8, bias64,
-    o8, l8, ob, lb, ro, rl, rlt, ri, rit, o1, l1, o2, l2,
+    o8, l8, ob, lb, ro, rlt, ri, rit, o1, l1, o2, l2, square,
     att, rb, rv,
     loc_sem, ag_send, ag_recv, dd_send, dd_recv, wo_send, wo_recv,
     xs_send, xs_recv, xq_send, xq_recv, z_send, z_recv, n_send, n_recv, ret_send, ret_recv,
@@ -110,6 +110,11 @@
     z_prev = (lax.rem(z + NZ - 1, NZ) * NX + x, tp)
     s_next = (lax.rem(sp + 1, NZ * NX), tp)
     s_prev = (lax.rem(sp + NZ * NX - 1, NZ * NX), tp)
+
+    has_up, has_down = z < NZ - 1, z > 0
+    has_both = has_up & has_down
+    has_up2, has_down2 = z < NZ - 2, z > 1
+    has_after, has_before = sp < NZ * NX - 1, sp > 0
 
     def remote(src, dst, ssem, rsem, dev):
         return pltpu.make_async_remote_copy(
@@ -130,9 +135,16 @@
     load_wo = pltpu.make_async_copy(wo_hbm, wo.at[c], loc_sem.at[6])
     load_wo.start()
     barrier = pltpu.get_barrier_semaphore()
-    for dev in [partner, y_next, y_prev, *x_peer[1:], z_next, z_prev, s_next, s_prev]:
+
+    def greet(dev):
         pl.semaphore_signal(barrier, inc=1, device_id=dev, device_id_type=MESH)
-    pl.semaphore_wait(barrier, 10)
+
+    for dev in [partner, y_next, y_prev, *x_peer[1:]]:
+        greet(dev)
+    for there, dev in ((has_up, z_next), (has_down, z_prev), (has_after, s_next), (has_before, s_prev)):
+        pl.when(there)(functools.partial(greet, dev))
+    ends = [there.astype(jnp.int32) for there in (has_up, has_down, has_after, has_before)]
+    pl.semaphore_wait(barrier, 6 + ends[0] + ends[1] + ends[2] + ends[3])
 
     top, low = pl.ds(0, SHARD // 2), pl.ds(SHARD // 2, SHARD // 2)
 
@@ -172,6 +184,14 @@
     ag[3].start()
     ag[1].start()
     ag[2].start()
+
+    for empty, ref in (
+        (z < 2, kv5.at[0]), (z < 1, kv5.at[1]), (z > NZ - 2, kv5.at[3]), (z > NZ - 3, kv5.at[4]),
+        (sp < 1, kvn.at[pl.ds(0, SHARD)]), (sp > NZ * NX - 2, kvn.at[pl.ds(ROWS + SHARD, SHARD)]),
+    ):
+        @pl.when(empty)
+        def _(ref=ref):
+            ref[...] = jnp.zeros(ref.shape, BF)
 
     r1 = iota((128, 256), 0)
     k1 = iota((128, 256), 1)
@@ -310,25 +330,25 @@
         for copy in kv_copies(slot):
             copy.wait_recv()
         for copies in z_copies(slot):
-            copies[0].start()
-            copies[1].start()
+            pl.when(has_up)(copies[0].start)
+            pl.when(has_down)(copies[1].start)
         for yc, half in slots[slot]:
             sort_half(2, yc, half)
 
     def z_forward(slot):
         for copies in z_copies(slot):
-            copies[0].wait_recv()
-            copies[2].start()
-            copies[1].wait_recv()
-            copies[3].start()
+            pl.when(has_down)(copies[0].wait_recv)
+            pl.when(has_both)(copies[2].start)
+            pl.when(has_up)(copies[1].wait_recv)
+            pl.when(has_both)(copies[3].start)
         for yc, half in slots[slot]:
             sort_half(1, yc, half)
             sort_half(3, yc, half)
 
     def z_finish(slot):
         for copies in z_copies(slot):
-            copies[2].wait_recv()
-            copies[3].wait_recv()
+            pl.when(has_down2)(copies[2].wait_recv)
+            pl.when(has_up2)(copies[3].wait_recv)
         for yc, half in slots[slot]:
             sort_half(0, yc, half)
             sort_half(4, yc, half)
@@ -354,13 +374,13 @@
 
     dd[0].wait_recv()
     project(0)
+    z_start(0)
     ag[0].wait_recv()
     ag[4].start()
     dd[1].start()
     ag[3].wait_recv()
     ag[5].start()
     dd[2].start()
-    z_start(0)
     share_wo = remote(wo_hbm, wo.at[c], wo_send, wo_recv, partner)
     dd[1].wait_recv()
     dd[2].wait_recv()
@@ -370,16 +390,16 @@
     dd[3].start()
     ag[2].wait_recv()
     dd[4].start()
+    z_start(1)
     dd[3].wait_recv()
     dd[4].wait_recv()
     project(2)
-    z_start(1)
     ag[4].wait_recv()
     dd[5].start()
     ag[5].wait_recv()
     dd[6].start()
-    share_wo.start()
     z_forward(1)
+    z_start(2)
     dd[5].wait_recv()
     dd[6].wait_recv()
     project(3)
@@ -387,15 +407,15 @@
         remote(kvn.at[pl.ds(ROWS, SHARD)], kvn.at[pl.ds(0, SHARD)], n_send.at[0], n_recv.at[0], s_next),
         remote(kvn.at[pl.ds(SHARD, SHARD)], kvn.at[pl.ds(ROWS + SHARD, SHARD)], n_send.at[1], n_recv.at[1], s_prev),
     ]
-    halo[0].start()
-    halo[1].start()
-    z_start(2)
+    pl.when(has_after)(halo[0].start)
+    pl.when(has_before)(halo[1].start)
+    share_wo.start()
     block1(1)
     block1(2)
     z_start(3)
     z_forward(2)
-    halo[0].wait_recv()
-    halo[1].wait_recv()
+    pl.when(has_before)(halo[0].wait_recv)
+    pl.when(has_after)(halo[1].wait_recv)
     block1(0)
     block1(3)
     for slot in range(4):
@@ -419,15 +439,15 @@
         o8[:, rows, :] = out.reshape(8, 16, COLS)
         l8[:, rows, :] = sums.reshape(8, 16, 128)
 
-    def two(block):
+    def several(block, count):
         def body(i, carry):
-            block(i * 2)
-            block(i * 2 + 1)
+            for n in range(count):
+                block(i * count + n)
             return carry
 
         return body
 
-    lax.fori_loop(0, 2, two(block8), 0)
+    lax.fori_loop(0, 2, several(block8, 2), 0)
     for slot in range(4):
         z_finish(slot)
 
@@ -440,9 +460,10 @@
         ob[:, half, rows, :] = out.astype(BF).reshape(4, 16, COLS)
         lb[:, half, rows, :] = sums.reshape(4, 16, 128)
 
-    lax.fori_loop(0, 4, two(block64), 0)
-
-    def join(i):
+    lax.fori_loop(0, 2, several(block64, 4), 0)
+
+    def join(k):
+        i = up_y(k)
         out64 = jnp.dot(swap_b, ob[i].reshape(128, COLS), preferred_element_type=F32)
         lse64 = jnp.dot(swap_f, lb[i].reshape(128, 128), preferred_element_type=F32, precision=lax.Precision.HIGHEST)
         two_halves = pl.ds(i * 2, 2)
@@ -450,64 +471,69 @@
             o8[two_halves].reshape(128, COLS), l8[two_halves].reshape(128, 128), out64, lse64
         )
         out = out.astype(BF)
-        for half in range(2):
-            rows = pl.ds(pl.multiple_of(i * 32 + half * 16, 16), 16)
-            ro[:, rows, :] = out[half * 64 : half * 64 + 64].reshape(4, 16, COLS)
-            rl[:, rows, :] = sums[half * 64 : half * 64 + 64].reshape(4, 16, 128)
-
-    lax.fori_loop(0, 2, two(join), 0)
-    for i in range(4):
-        rlt[i] = rl[i].T[0:8, :]
+        parts = []
+        for n in range(4):
+            for half in range(2):
+                at = slice(half * 64 + n * 16, half * 64 + n * 16 + 16)
+                ro[k, n, half * 16 : half * 16 + 16, :] = out[at]
+                parts.append(sums[at])
+        rlt[k] = jnp.concatenate(parts, axis=0).T[0:8, :]
+        ri[k, x] = ro[k, x]
+        rit[k, x] = rlt[k]
+
+    def back_copies(k):
+        out = []
+        for d in (2, 1, 3):
+            to = lax.rem(x + d, NX)
+            out.append(remote(ro.at[k, to], ri.at[k, x], ret_send.at[k, d - 1, 0], ret_recv.at[k, d - 1, 0], x_peer[d]))
+            out.append(remote(rlt.at[k], rit.at[k, x], ret_send.at[k, d - 1, 1], ret_recv.at[k, d - 1, 1], x_peer[d]))
+        return out
+
     backs = []
-    for d in (2, 1, 3):
-        to = lax.rem(x + d, NX)
-        backs.append(remote(ro.at[to], ri.at[x], ret_send.at[d - 1, 0], ret_recv.at[d - 1, 0], x_peer[d]))
-        backs.append(remote(rlt.at[to], rit.at[x], ret_send.at[d - 1, 1], ret_recv.at[d - 1, 1], x_peer[d]))
-    for copy in backs:
-        copy.start()
-    ri[x] = ro[x]
-    rit[x] = rlt[x]
-    for copy in backs:
-        copy.wait_recv()
-    for i in range(4):
-        o = ri[i].astype(F32)
-        square = jnp.concatenate([rit[i], jnp.zeros((120, 128), F32)], axis=0).T
-        for m in range(16):
-            at = (m // 4) * 128 + (m % 4 // 2) * 32 + (m % 2) * 64 + i
-            part = slice(m * 8, m * 8 + 8)
-            for n in range(2):
-                o2[n, pl.ds(at, 8, stride=4), :] = o[part, n * 128 : (n + 1) * 128]
-            l2[pl.ds(at, 8, stride=4), :] = square[part]
-
-    def last(i):
-        rows = slice(i * 128, (i + 1) * 128)
-        wide = jnp.concatenate([o2[0, rows, :], o2[1, rows, :]], axis=1)
-        out, sums = merge(o1[rows, :], l1[rows, :], wide, l2[rows, :])
-        att[c, i * 2 : i * 2 + 2] = out.astype(BF).reshape(2, SHARD, COLS)
+    for k in (2, 1, 3, 0):
+        join(k)
+        for copy in back_copies(k):
+            copy.start()
+            backs.append(copy)
+
+    def trade_copy(k):
+        u = up_y(k) * 2 + other
+        return remote(att.at[c, u], att.at[c, u], at_send.at[k], at_recv.at[k], partner)
+
+    def settle(k):
+        yc = up_y(k)
+        for copy in back_copies(k):
+            copy.wait_recv()
+        for i in range(4):
+            o = ri[k, i].astype(F32)
+            square[...] = jnp.concatenate([rit[k, i], jnp.zeros((120, 128), F32)], axis=0).T
+            sums = square[pl.ds(pl.multiple_of(x * 32, 32), 32), :]
+            for m in range(4):
+                at = (m // 2) * 32 + (m % 2) * 64 + i
+                part = slice(m * 8, m * 8 + 8)
+                for n in range(2):
+                    o2[n, pl.ds(at, 8, stride=4), :] = o[part, n * 128 : (n + 1) * 128]
+                l2[pl.ds(at, 8, stride=4), :] = sums[part]
+        rows = pl.ds(pl.multiple_of(yc * 128, 128), 128)
+        wide = jnp.concatenate([o2[0], o2[1]], axis=1)
+        out, sums = merge(o1[rows, :], l1[rows, :], wide, l2[...])
+        att[c, pl.ds(yc * 2, 2)] = out.astype(BF).reshape(2, SHARD, COLS)
         logw_ref[:, rows] = sums.T[0:4, :]
-
-    for i in range(4):
-        last(i)
-
-    trade = []
-    for k in range(4):
-        u = up_y(k) * 2 + other
-        trade.append(remote(att.at[c, u], att.at[c, u], at_send.at[k], at_recv.at[k], partner))
-    for copy in trade:
-        copy.start()
-    load_wo.wait()
-    share_wo.wait_recv()
-    for copy in trade:
-        copy.wait_recv()
-    lhs = [
-        jnp.concatenate([att[i, up_y(k) * 2 + c] for k in range(4)], axis=0) for i in range(2)
-    ]
-
-    def columns(n):
+        trade_copy(k).start()
+
+    def gather_rows(group):
+        for k in group:
+            trade_copy(k).wait_recv()
+        return [
+            jnp.concatenate([att[i, up_y(k) * 2 + c] for k in group], axis=0) for i in range(2)
+        ]
+
+    def columns(group, lhs, n):
         cols = slice(n * 512, (n + 1) * 512)
         acc = jnp.dot(lhs[0], wo[0, :, cols], preferred_element_type=F32)
         acc = acc + jnp.dot(lhs[1], wo[1, :, cols], preferred_element_type=F32)
-        rb[:, n] = acc.astype(BF).reshape(4, SHARD, 512)
+        for m, k in enumerate(group):
+            rb[k, n] = acc[m * SHARD : (m + 1) * SHARD].astype(BF)
 
     def rs(i, n, src, dev):
         return remote(rb.at[src, n], rv.at[i, n // 2], rs_send.at[i, n // 2], rs_recv.at[i, n // 2], dev)
@@ -520,16 +546,25 @@
     direct_p = {n: rs(3, n, 3, y_prev) for n in even}
     sum_n = {n: rs(4, n, 1, y_next) for n in even}
     sum_p = {n: rs(5, n, 3, y_prev) for n in odd}
+    settle(2)
+    load_wo.wait()
+    share_wo.wait_recv()
+    lhs = gather_rows((2,))
     for n in range(8):
-        columns(n)
+        columns((2,), lhs, n)
         if n % 2 == 0:
             first_n[n].start()
         else:
             first_p[n].start()
-    for n in range(0, 8, 2):
-        direct_n[n + 1].start()
-        direct_p[n].start()
-
+    settle(1)
+    settle(3)
+    lhs = gather_rows((1, 3))
+    for n in range(8):
+        columns((1, 3), lhs, n)
+        if n % 2 == 0:
+            direct_p[n].start()
+        else:
+            direct_n[n].start()
     for n in range(0, 8, 2):
         first_n[n].wait_recv()
         rb[1, n] = (rb[1, n].astype(F32) + rv[0, n // 2].astype(F32)).astype(BF)
@@ -537,6 +572,10 @@
         first_p[n + 1].wait_recv()
         rb[3, n + 1] = (rb[3, n + 1].astype(F32) + rv[1, n // 2].astype(F32)).astype(BF)
         sum_p[n + 1].start()
+    settle(0)
+    lhs = gather_rows((0,))
+    for n in range(8):
+        columns((0,), lhs, n)
     for n in range(0, 8, 2):
         direct_n[n + 1].wait_recv()
         direct_p[n].wait_recv()
@@ -547,8 +586,10 @@
         acc = acc + rv[4 if n % 2 == 0 else 5, n // 2].astype(F32)
         mixed_ref[:, n * 512 : (n + 1) * 512] = acc.astype(BF)
 
-    for copy in ag + dd + [share_wo] + halo + backs + trade:
+    for copy in ag + dd + [share_wo] + backs + [trade_copy(k) for k in range(4)]:
         copy.wait_send()
+    pl.when(has_after)(halo[0].wait_send)
+    pl.when(has_before)(halo[1].wait_send)
     for group in (first_n, first_p, direct_n, direct_p, sum_n, sum_p):
         for copy in group.values():
             copy.wait_send()
@@ -556,8 +597,10 @@
         for copy in kv_copies(slot) + q_copies(slot):
             copy.wait_send()
         for copies in z_copies(slot):
-            for copy in copies:
-                copy.wait_send()
+            pl.when(has_up)(copies[0].wait_send)
+            pl.when(has_down)(copies[1].wait_send)
+            pl.when(has_both)(copies[2].wait_send)
+            pl.when(has_both)(copies[3].wait_send)
 
 
 def per_device(tokens_in, w_query, w_key, w_value, w_out):
@@ -586,15 +629,15 @@
         vm((8, 64, 128), F32),
         vm((4, 2, 64, COLS), BF),
         vm((4, 2, 64, 128), F32),
-        vm((4, 128, COLS), BF),
-        vm((4, 128, 128), F32),
+        vm((4, 4, 32, COLS), BF),
         vm((4, 8, 128), F32),
-        vm((4, 128, COLS), BF),
-        vm((4, 8, 128), F32),
+        vm((4, 4, 32, COLS), BF),
+        vm((4, 4, 8, 128), F32),
         vm((ROWS, COLS), F32),
         vm((ROWS, 128), F32),
-        vm((2, ROWS, 128), F32),
-        vm((ROWS, 128), F32),
+        vm((2, 128, 128), F32),
+        vm((128, 128), F32),
+        vm((128, 128), F32),
         vm((2, 8, SHARD, COLS), BF),
         vm((4, 8, SHARD, 512), BF),
         vm((6, 4, SHARD, 512), BF),
@@ -606,7 +649,7 @@
         dma((4, 3, 2)), dma((4, 3, 2)),
         dma((4, 2, 4)), dma((4, 2, 4)),
         dma((2,)), dma((2,)),
-        dma((3, 2)), dma((3, 2)),
+        dma((4, 3, 2)), dma((4, 3, 2)),
         dma((4,)), dma((4,)),
         dma((6, 4)), dma((6, 4)),
     ]

time: 86.6 us -> 77.6 us (0.90)
  Pallas kernels: 82.7 us -> 73.5 us
    pallas_call x1, Pallas kernels: 82.7 us -> 73.5 us  [per_device(): pl.pallas_call(kernel, out_shape=(jax.ShapeDtypeStruct((SHARD, D), BF), j...]
where the time goes in v2:
time: 77.6 us; the launch traced here: 77.3 us
  Pallas kernels  73.5 us (95%)
  local copies, waits for them, and re-layouts  3.16 us (4%)
    pallas_call x1, Pallas kernels, per_device(): pl.pallas_call(kernel, out_shape=(jax.ShapeDtypeStruct((SHARD, D), BF), j...  73.5 us
    unnamed x2, local copies, waits for them, and re-layouts  3.16 us

profile of v2, /device:TPU:1, one launch (start us, length us, event | category | flops | bytes accessed | tf_op | source)
XLA Modules:
  0.0 77.3 jit_solution(14940816675221018979)
XLA Ops:
  0.6 73.5 %shard_map.86 = (bf16[64,4096]{1,0:T(8,128)(2,1)}, f32[4,512]{1,0:T(4,128)}) custom-call(bf16[64,4096]{1,0:T(8,128)(2,1)} %x_hbm.1, bf16[4096,256]{1,0:T(8,128)(2,1)} %wq_hbm.1, bf16[4096,256]{1,0:T(8,128)(2,1)} %wk_hbm.1, bf16[4096,256]{1,0:T(8,128)(2,1)} %wv_hbm.1, bf16[256,4096]{1,0:T(8,128)(2,1)} %wo_hbm.1, f32[2,64,128]{2,1,0:T(8,128)} %constant.4.clone.near_hbm, ...), custom_call_target="tpu_custom_call" | custom-call | tf_op jit(solution)/shard_map/pallas_call | solution.py:658
  74.1 1.9 %copy.11 = bf16[64,4096]{1,0:T(8,128)(2,1)} copy(bf16[64,4096]{1,0:T(8,128)(2,1)} %get-tuple-element.4) | data formatting | bytes 1048576
  76.0 1.3 %copy.12 = f32[4,512]{1,0:T(4,128)} copy(f32[4,512]{1,0:T(4,128)} %get-tuple-element.5) | data formatting | bytes 16384

commit v3 on v2

--- a/solution.py
+++ b/solution.py
@@ -14,6 +14,10 @@
 D = 4096
 COLS = 256
 SIDE = 64
+PIECES = ((0, 640), (640, 640), (1280, 640), (1920, 640))
+WIDEST = 640
+RING = 2560
+REST = (D - RING) // 2
 TOKENS = 16384
 ROTARY_BASE = 500000.0
 NEG = -1e30
@@ -86,10 +90,11 @@
     rot, qn, kvn, send_q, send_kv, qa, kv5, qb, kvb,
     bias1, bias8, bias64,
     o8, l8, ob, lb, ro, rlt, ri, rit, o1, l1, o2, l2, square,
-    att, rb, rv,
+    att, rb, rv, wg, relay, attg, gout, gin,
     loc_sem, ag_send, ag_recv, dd_send, dd_recv, wo_send, wo_recv,
     xs_send, xs_recv, xq_send, xq_recv, z_send, z_recv, n_send, n_recv, ret_send, ret_recv,
     at_send, at_recv, rs_send, rs_recv,
+    wg_send, wg_recv, sp_send, sp_recv, pass_send, pass_recv, give_send, give_recv,
 ):
     sp = lax.axis_index("sp")
     tp = lax.axis_index("tp")
@@ -132,8 +137,15 @@
     ]
     for copy in loads:
         copy.start()
-    load_wo = pltpu.make_async_copy(wo_hbm, wo.at[c], loc_sem.at[6])
-    load_wo.start()
+    ring_cols = pl.ds(0, RING)
+    own_cols = pl.ds(pl.multiple_of(RING + c * REST, 128), REST)
+    other_cols = pl.ds(pl.multiple_of(RING + other * REST, 128), REST)
+    load_wo = [
+        pltpu.make_async_copy(wo_hbm.at[:, own_cols], wg.at[0, c], loc_sem.at[6]),
+        pltpu.make_async_copy(wo_hbm.at[:, ring_cols], wo.at[c], loc_sem.at[7]),
+    ]
+    for copy in load_wo:
+        copy.start()
     barrier = pltpu.get_barrier_semaphore()
 
     def greet(dev):
@@ -374,6 +386,12 @@
 
     dd[0].wait_recv()
     project(0)
+    share_wo = [
+        remote(wo_hbm.at[:, other_cols], wg.at[0, c], wo_send.at[0], wo_recv.at[0], partner),
+        remote(wo_hbm.at[:, ring_cols], wo.at[c], wo_send.at[1], wo_recv.at[1], partner),
+    ]
+    for copy in share_wo:
+        copy.start()
     z_start(0)
     ag[0].wait_recv()
     ag[4].start()
@@ -381,7 +399,6 @@
     ag[3].wait_recv()
     ag[5].start()
     dd[2].start()
-    share_wo = remote(wo_hbm, wo.at[c], wo_send, wo_recv, partner)
     dd[1].wait_recv()
     dd[2].wait_recv()
     project(1)
@@ -398,6 +415,19 @@
     dd[5].start()
     ag[5].wait_recv()
     dd[6].start()
+    wgs = [
+        remote(wg.at[a, i], wg.at[b, i], wg_send.at[n], wg_recv.at[n], dev)
+        for n, (a, b, i, dev) in enumerate(
+            [
+                (0, 3, 0, y_next), (0, 3, 1, y_next), (0, 1, 0, y_prev), (0, 1, 1, y_prev),
+                (3, 2, 0, y_next), (1, 2, 1, y_prev),
+            ]
+        )
+    ]
+    load_wo[0].wait()
+    share_wo[0].wait_recv()
+    for n in (0, 3, 1, 2):
+        wgs[n].start()
     z_forward(1)
     z_start(2)
     dd[5].wait_recv()
@@ -409,7 +439,6 @@
     ]
     pl.when(has_after)(halo[0].start)
     pl.when(has_before)(halo[1].start)
-    share_wo.start()
     block1(1)
     block1(2)
     z_start(3)
@@ -447,6 +476,10 @@
 
         return body
 
+    wgs[0].wait_recv()
+    wgs[4].start()
+    wgs[3].wait_recv()
+    wgs[5].start()
     lax.fori_loop(0, 2, several(block8, 2), 0)
     for slot in range(4):
         z_finish(slot)
@@ -497,8 +530,22 @@
             backs.append(copy)
 
     def trade_copy(k):
-        u = up_y(k) * 2 + other
+        u = up_y(k) * 2 + other if k else pl.ds(y * 2, 2)
         return remote(att.at[c, u], att.at[c, u], at_send.at[k], at_recv.at[k], partner)
+
+    both = pl.ds(0, 2)
+    to_far = up_y(2) * 2 + c
+    spread = [
+        remote(att.at[0, to_far], relay.at[0], sp_send.at[0], sp_recv.at[0], y_next),
+        remote(att.at[1, to_far], relay.at[1], sp_send.at[1], sp_recv.at[1], y_prev),
+        remote(relay.at[0], attg.at[c, 2, 0], sp_send.at[2], sp_recv.at[2], y_next),
+        remote(relay.at[1], attg.at[c, 2, 1], sp_send.at[3], sp_recv.at[3], y_prev),
+        remote(att.at[both, up_y(1) * 2 + c], attg.at[c, 3], sp_send.at[4], sp_recv.at[4], y_next),
+        remote(att.at[both, up_y(3) * 2 + c], attg.at[c, 1], sp_send.at[5], sp_recv.at[5], y_prev),
+    ]
+    pass_on = [
+        remote(attg.at[c, r], attg.at[c, r], pass_send.at[r - 1], pass_recv.at[r - 1], partner) for r in (1, 2, 3)
+    ]
 
     def settle(k):
         yc = up_y(k)
@@ -529,17 +576,21 @@
         ]
 
     def columns(group, lhs, n):
-        cols = slice(n * 512, (n + 1) * 512)
+        start, width = PIECES[n]
+        cols = slice(start, start + width)
         acc = jnp.dot(lhs[0], wo[0, :, cols], preferred_element_type=F32)
         acc = acc + jnp.dot(lhs[1], wo[1, :, cols], preferred_element_type=F32)
         for m, k in enumerate(group):
-            rb[k, n] = acc[m * SHARD : (m + 1) * SHARD].astype(BF)
+            rb[k, n, :, 0:width] = acc[m * SHARD : (m + 1) * SHARD].astype(BF)
 
     def rs(i, n, src, dev):
-        return remote(rb.at[src, n], rv.at[i, n // 2], rs_send.at[i, n // 2], rs_recv.at[i, n // 2], dev)
-
-    even = range(0, 8, 2)
-    odd = range(1, 8, 2)
+        cols = pl.ds(0, PIECES[n][1])
+        return remote(
+            rb.at[src, n, :, cols], rv.at[i, n // 2, :, cols], rs_send.at[i, n // 2], rs_recv.at[i, n // 2], dev
+        )
+
+    even = range(0, len(PIECES), 2)
+    odd = range(1, len(PIECES), 2)
     first_n = {n: rs(0, n, 2, y_next) for n in even}
     first_p = {n: rs(1, n, 2, y_prev) for n in odd}
     direct_n = {n: rs(2, n, 1, y_next) for n in odd}
@@ -547,10 +598,12 @@
     sum_n = {n: rs(4, n, 1, y_next) for n in even}
     sum_p = {n: rs(5, n, 3, y_prev) for n in odd}
     settle(2)
-    load_wo.wait()
-    share_wo.wait_recv()
+    load_wo[1].wait()
+    share_wo[1].wait_recv()
     lhs = gather_rows((2,))
-    for n in range(8):
+    spread[0].start()
+    spread[1].start()
+    for n in range(len(PIECES)):
         columns((2,), lhs, n)
         if n % 2 == 0:
             first_n[n].start()
@@ -558,35 +611,66 @@
             first_p[n].start()
     settle(1)
     settle(3)
+    spread[0].wait_recv()
+    spread[2].start()
+    spread[1].wait_recv()
+    spread[3].start()
     lhs = gather_rows((1, 3))
-    for n in range(8):
+    for n in range(len(PIECES)):
         columns((1, 3), lhs, n)
         if n % 2 == 0:
             direct_p[n].start()
         else:
             direct_n[n].start()
-    for n in range(0, 8, 2):
+    spread[4].start()
+    spread[5].start()
+    for n in even:
+        width = PIECES[n][1]
         first_n[n].wait_recv()
-        rb[1, n] = (rb[1, n].astype(F32) + rv[0, n // 2].astype(F32)).astype(BF)
+        rb[1, n, :, 0:width] = (rb[1, n, :, 0:width].astype(F32) + rv[0, n // 2, :, 0:width].astype(F32)).astype(BF)
         sum_n[n].start()
+        width = PIECES[n + 1][1]
         first_p[n + 1].wait_recv()
-        rb[3, n + 1] = (rb[3, n + 1].astype(F32) + rv[1, n // 2].astype(F32)).astype(BF)
+        rb[3, n + 1, :, 0:width] = (
+            rb[3, n + 1, :, 0:width].astype(F32) + rv[1, n // 2, :, 0:width].astype(F32)
+        ).astype(BF)
         sum_p[n + 1].start()
     settle(0)
     lhs = gather_rows((0,))
-    for n in range(8):
+    for n in range(len(PIECES)):
         columns((0,), lhs, n)
-    for n in range(0, 8, 2):
+    spread[5].wait_recv()
+    pass_on[0].start()
+    spread[4].wait_recv()
+    pass_on[2].start()
+    spread[2].wait_recv()
+    spread[3].wait_recv()
+    pass_on[1].start()
+    for n in (1, 2, 4, 5):
+        wgs[n].wait_recv()
+    for copy in pass_on:
+        copy.wait_recv()
+    rows = [jnp.concatenate([att[i, y * 2], att[i, y * 2 + 1]], axis=0) for i in range(2)]
+    rows += [jnp.concatenate([attg[0, r, i], attg[1, r, i]], axis=0) for r in (1, 2, 3) for i in range(2)]
+    acc = jnp.dot(jnp.concatenate(rows, axis=1), wg[...].reshape(8 * COLS, REST), preferred_element_type=F32)
+    gout[...] = acc.astype(BF).reshape(2, SHARD, REST)
+    give = remote(gout.at[other], gin, give_send, give_recv, partner)
+    give.start()
+    mixed_ref[:, own_cols] = gout[c]
+    for n in even:
         direct_n[n + 1].wait_recv()
         direct_p[n].wait_recv()
-    for n in range(8):
-        one, other_one = ((direct_p, sum_n) if n % 2 == 0 else (direct_n, sum_p))
-        other_one[n].wait_recv()
-        acc = rb[0, n].astype(F32) + rv[3 if n % 2 == 0 else 2, n // 2].astype(F32)
-        acc = acc + rv[4 if n % 2 == 0 else 5, n // 2].astype(F32)
-        mixed_ref[:, n * 512 : (n + 1) * 512] = acc.astype(BF)
-
-    for copy in ag + dd + [share_wo] + backs + [trade_copy(k) for k in range(4)]:
+    for n in range(len(PIECES)):
+        start, width = PIECES[n]
+        (sum_n if n % 2 == 0 else sum_p)[n].wait_recv()
+        acc = rb[0, n, :, 0:width].astype(F32) + rv[3 if n % 2 == 0 else 2, n // 2, :, 0:width].astype(F32)
+        acc = acc + rv[4 if n % 2 == 0 else 5, n // 2, :, 0:width].astype(F32)
+        mixed_ref[:, start : start + width] = acc.astype(BF)
+    give.wait_recv()
+    mixed_ref[:, other_cols] = gin[...]
+
+    trades = [trade_copy(k) for k in range(4)]
+    for copy in ag + dd + share_wo + wgs + backs + trades + spread + pass_on + [give]:
         copy.wait_send()
     pl.when(has_after)(halo[0].wait_send)
     pl.when(has_before)(halo[1].wait_send)
@@ -603,6 +687,22 @@
             pl.when(has_both)(copies[3].wait_send)
 
 
+def hand_on(mixed_in, logw_in, mixed_out, logw_out, mixed_vm, logw_vm, sems):
+    reads, writes = [], []
+    for i in range(3):
+        part = pl.ds(i * 32, 32) if i < 2 else slice(None)
+        src, mid, dst = (mixed_in, mixed_vm, mixed_out) if i < 2 else (logw_in, logw_vm, logw_out)
+        reads.append(pltpu.make_async_copy(src.at[part], mid.at[part], sems.at[i, 0]))
+        writes.append(pltpu.make_async_copy(mid.at[part], dst.at[part], sems.at[i, 1]))
+    for copy in reads:
+        copy.start()
+    for read, write in zip(reads, writes):
+        read.wait()
+        write.start()
+    for copy in writes:
+        copy.wait()
+
+
 def per_device(tokens_in, w_query, w_key, w_value, w_out):
     near, far = rotary_tables()
     dma = pltpu.SemaphoreType.DMA
@@ -610,7 +710,7 @@
     scratch = [
         vm((8, SHARD, D), BF),
         vm((3, D, COLS), BF),
-        vm((2, COLS, D), BF),
+        vm((2, COLS, RING), BF),
         vm((2, SHARD, 128), F32),
         vm((2, TOKENS // SHARD, 128), F32),
         vm((6, 128, 128), F32),
@@ -639,23 +739,32 @@
         vm((128, 128), F32),
         vm((128, 128), F32),
         vm((2, 8, SHARD, COLS), BF),
-        vm((4, 8, SHARD, 512), BF),
-        vm((6, 4, SHARD, 512), BF),
-        dma((7,)),
+        vm((4, len(PIECES), SHARD, WIDEST), BF),
+        vm((6, len(PIECES) // 2, SHARD, WIDEST), BF),
+        vm((4, 2, COLS, REST), BF),
+        vm((2, SHARD, COLS), BF),
+        vm((2, 4, 2, SHARD, COLS), BF),
+        vm((2, SHARD, REST), BF),
+        vm((SHARD, REST), BF),
+        dma((8,)),
         dma((6,)), dma((6,)),
         dma((7,)), dma((7,)),
-        dma(()), dma(()),
+        dma((2,)), dma((2,)),
         dma((4, 3, 2)), dma((4, 3, 2)),
         dma((4, 3, 2)), dma((4, 3, 2)),
         dma((4, 2, 4)), dma((4, 2, 4)),
         dma((2,)), dma((2,)),
         dma((4, 3, 2)), dma((4, 3, 2)),
         dma((4,)), dma((4,)),
-        dma((6, 4)), dma((6, 4)),
+        dma((6, len(PIECES) // 2)), dma((6, len(PIECES) // 2)),
+        dma((6,)), dma((6,)),
+        dma((6,)), dma((6,)),
+        dma((3,)), dma((3,)),
+        dma(()), dma(()),
     ]
     hbm = pl.BlockSpec(memory_space=pl.ANY)
     vmem = pl.BlockSpec(memory_space=pltpu.VMEM)
-    return pl.pallas_call(
+    mixed, logw = pl.pallas_call(
         kernel,
         out_shape=(jax.ShapeDtypeStruct((SHARD, D), BF), jax.ShapeDtypeStruct((4, ROWS), F32)),
         in_specs=[hbm] * 7,
@@ -665,6 +774,13 @@
             collective_id=0, has_side_effects=True, vmem_limit_bytes=60 * 1024 * 1024
         ),
     )(tokens_in, w_query, w_key, w_value, w_out, jnp.asarray(near), jnp.asarray(far))
+    return pl.pallas_call(
+        hand_on,
+        out_shape=(jax.ShapeDtypeStruct((SHARD, D), BF), jax.ShapeDtypeStruct((4, ROWS), F32)),
+        in_specs=[hbm, hbm],
+        out_specs=(hbm, hbm),
+        scratch_shapes=[vm((SHARD, D), BF), vm((4, ROWS), F32), dma((4, 2))],
+    )(mixed, logw)
 
 
 def solution(mesh):

time: 77.6 us -> 72.7 us (0.937)
  local copies, waits for them, and re-layouts: 3.16 us -> 0 us
  Pallas kernels: 73.5 us -> 71.6 us
    pallas_call x1, Pallas kernels: 73.5 us -> 69.8 us  [per_device(): pl.pallas_call(kernel, out_shape=(jax.ShapeDtypeStruct((SHARD, D), BF), j...]
    unnamed x2 -> x0, local copies, waits for them, and re-layouts: 3.16 us -> none
    pallas_call x0 -> x1, Pallas kernels: none -> 1.81 us  [per_device(): pl.pallas_call(hand_on, out_shape=(jax.ShapeDtypeStruct((SHARD, D), BF),...]
where the time goes in v3:
time: 72.7 us; the launch traced here: 72.4 us
  Pallas kernels  71.6 us (98%)
  between operations  0.8 us (1%)
    pallas_call x1, Pallas kernels, per_device(): pl.pallas_call(kernel, out_shape=(jax.ShapeDtypeStruct((SHARD, D), BF), j...  69.8 us
    pallas_call x1, Pallas kernels, per_device(): pl.pallas_call(hand_on, out_shape=(jax.ShapeDtypeStruct((SHARD, D), BF),...  1.81 us

profile of v3, /device:TPU:1, one launch (start us, length us, event | category | flops | bytes accessed | tf_op | source)
XLA Modules:
  0.0 72.4 jit_solution(16619283604538950177)
XLA Ops:
  0.6 69.8 %shard_map.86 = (bf16[64,4096]{1,0:T(8,128)(2,1)}, f32[4,512]{1,0:T(4,128)}) custom-call(bf16[64,4096]{1,0:T(8,128)(2,1)} %x_hbm.1, bf16[4096,256]{1,0:T(8,128)(2,1)} %wq_hbm.1, bf16[4096,256]{1,0:T(8,128)(2,1)} %wk_hbm.1, bf16[4096,256]{1,0:T(8,128)(2,1)} %wv_hbm.1, bf16[256,4096]{1,0:T(8,128)(2,1)} %wo_hbm.1, f32[2,64,128]{2,1,0:T(8,128)} %constant.4.clone.near_hbm, ...), custom_call_target="tpu_custom_call" | custom-call | tf_op jit(solution)/shard_map/pallas_call | solution.py:767
  70.4 1.8 %shard_map.87 = (bf16[64,4096]{1,0:T(8,128)(2,1)}, f32[4,512]{1,0:T(4,128)}) custom-call(bf16[64,4096]{1,0:T(8,128)(2,1)} %get-tuple-element.4.mixed_in, f32[4,512]{1,0:T(4,128)} %get-tuple-element.5.logw_in), custom_call_target="tpu_custom_call" | custom-call | tf_op jit(solution)/shard_map/pallas_call | solution.py:777

commit v4 on v3

--- a/solution.py
+++ b/solution.py
@@ -14,10 +14,12 @@
 D = 4096
 COLS = 256
 SIDE = 64
-PIECES = ((0, 640), (640, 640), (1280, 640), (1920, 640))
-WIDEST = 640
-RING = 2560
+PIECES = ((0, 512), (512, 512), (1024, 384), (1408, 384))
+WIDEST = 512
+RING = 1792
 REST = (D - RING) // 2
+QUARTER = 128
+ALONE = REST - 4 * QUARTER
 TOKENS = 16384
 ROTARY_BASE = 500000.0
 NEG = -1e30
@@ -90,11 +92,11 @@
     rot, qn, kvn, send_q, send_kv, qa, kv5, qb, kvb,
     bias1, bias8, bias64,
     o8, l8, ob, lb, ro, rlt, ri, rit, o1, l1, o2, l2, square,
-    att, rb, rv, wg, relay, attg, gout, gin,
+    att, rb, rv, wg, relay, attg, gacc, gout, gin,
     loc_sem, ag_send, ag_recv, dd_send, dd_recv, wo_send, wo_recv,
     xs_send, xs_recv, xq_send, xq_recv, z_send, z_recv, n_send, n_recv, ret_send, ret_recv,
     at_send, at_recv, rs_send, rs_recv,
-    wg_send, wg_recv, sp_send, sp_recv, pass_send, pass_recv, give_send, give_recv,
+    wg_send, wg_recv, wx_send, wx_recv, sp_send, sp_recv, pass_send, pass_recv, give_send, give_recv,
 ):
     sp = lax.axis_index("sp")
     tp = lax.axis_index("tp")
@@ -138,12 +140,20 @@
     for copy in loads:
         copy.start()
     ring_cols = pl.ds(0, RING)
-    own_cols = pl.ds(pl.multiple_of(RING + c * REST, 128), REST)
-    other_cols = pl.ds(pl.multiple_of(RING + other * REST, 128), REST)
+
+    def whole_cols(core):
+        base = RING + core * REST
+        parts = [(pl.ds(pl.multiple_of(base + 4 * QUARTER, 128), ALONE), pl.ds(0, ALONE))]
+        for r in range(4):
+            start = pl.multiple_of(base + lax.rem(x + r, NX) * QUARTER, 128)
+            parts.append((pl.ds(start, QUARTER), pl.ds(ALONE + r * QUARTER, QUARTER)))
+        return parts
+
     load_wo = [
-        pltpu.make_async_copy(wo_hbm.at[:, own_cols], wg.at[0, c], loc_sem.at[6]),
-        pltpu.make_async_copy(wo_hbm.at[:, ring_cols], wo.at[c], loc_sem.at[7]),
-    ]
+        pltpu.make_async_copy(wo_hbm.at[:, there], wg.at[0, c, :, here], loc_sem.at[6 + n])
+        for n, (there, here) in enumerate(whole_cols(c))
+    ]
+    load_wo.append(pltpu.make_async_copy(wo_hbm.at[:, ring_cols], wo.at[c], loc_sem.at[11]))
     for copy in load_wo:
         copy.start()
     barrier = pltpu.get_barrier_semaphore()
@@ -387,9 +397,10 @@
     dd[0].wait_recv()
     project(0)
     share_wo = [
-        remote(wo_hbm.at[:, other_cols], wg.at[0, c], wo_send.at[0], wo_recv.at[0], partner),
-        remote(wo_hbm.at[:, ring_cols], wo.at[c], wo_send.at[1], wo_recv.at[1], partner),
-    ]
+        remote(wo_hbm.at[:, there], wg.at[0, c, :, here], wo_send.at[n], wo_recv.at[n], partner)
+        for n, (there, here) in enumerate(whole_cols(other))
+    ]
+    share_wo.append(remote(wo_hbm.at[:, ring_cols], wo.at[c], wo_send.at[5], wo_recv.at[5], partner))
     for copy in share_wo:
         copy.start()
     z_start(0)
@@ -415,19 +426,39 @@
     dd[5].start()
     ag[5].wait_recv()
     dd[6].start()
-    wgs = [
-        remote(wg.at[a, i], wg.at[b, i], wg_send.at[n], wg_recv.at[n], dev)
+    def gather_copies(cols, first):
+        return [
+            remote(wg.at[a, i, :, cols], wg.at[b, i, :, cols], wg_send.at[first + n], wg_recv.at[first + n], dev)
+            for n, (a, b, i, dev) in enumerate(
+                [
+                    (0, 3, 0, y_next), (0, 3, 1, y_next), (0, 1, 0, y_prev), (0, 1, 1, y_prev),
+                    (3, 2, 0, y_next), (1, 2, 1, y_prev),
+                ]
+            )
+        ]
+
+    wq = gather_copies(pl.ds(ALONE, QUARTER), 0)
+    wy = gather_copies(pl.ds(0, ALONE), 6)
+    others = pl.ds(1, 3)
+
+    def quarter(r):
+        return pl.ds(ALONE + r * QUARTER, QUARTER)
+
+    x_next, x_prev = x_peer[1], x_peer[3]
+    wx = [
+        remote(wg.at[others, i, :, quarter(a)], wg.at[others, i, :, quarter(b)], wx_send.at[n], wx_recv.at[n], dev)
         for n, (a, b, i, dev) in enumerate(
             [
-                (0, 3, 0, y_next), (0, 3, 1, y_next), (0, 1, 0, y_prev), (0, 1, 1, y_prev),
-                (3, 2, 0, y_next), (1, 2, 1, y_prev),
+                (0, 3, 0, x_next), (0, 3, 1, x_next), (0, 1, 0, x_prev), (0, 1, 1, x_prev),
+                (3, 2, 0, x_next), (1, 2, 1, x_prev),
             ]
         )
     ]
-    load_wo[0].wait()
-    share_wo[0].wait_recv()
+    for n in range(5):
+        load_wo[n].wait()
+        share_wo[n].wait_recv()
     for n in (0, 3, 1, 2):
-        wgs[n].start()
+        wq[n].start()
     z_forward(1)
     z_start(2)
     dd[5].wait_recv()
@@ -439,10 +470,20 @@
     ]
     pl.when(has_after)(halo[0].start)
     pl.when(has_before)(halo[1].start)
+    wq[0].wait_recv()
+    wq[4].start()
+    wq[3].wait_recv()
+    wq[5].start()
+    for n in (0, 3, 1, 2):
+        wy[n].start()
     block1(1)
     block1(2)
     z_start(3)
     z_forward(2)
+    for n in (1, 2, 4, 5):
+        wq[n].wait_recv()
+    for n in (0, 3, 1, 2):
+        wx[n].start()
     pl.when(has_before)(halo[0].wait_recv)
     pl.when(has_after)(halo[1].wait_recv)
     block1(0)
@@ -476,10 +517,6 @@
 
         return body
 
-    wgs[0].wait_recv()
-    wgs[4].start()
-    wgs[3].wait_recv()
-    wgs[5].start()
     lax.fori_loop(0, 2, several(block8, 2), 0)
     for slot in range(4):
         z_finish(slot)
@@ -493,6 +530,10 @@
         ob[:, half, rows, :] = out.astype(BF).reshape(4, 16, COLS)
         lb[:, half, rows, :] = sums.reshape(4, 16, 128)
 
+    wy[0].wait_recv()
+    wy[4].start()
+    wy[3].wait_recv()
+    wy[5].start()
     lax.fori_loop(0, 2, several(block64, 4), 0)
 
     def join(k):
@@ -528,6 +569,11 @@
         for copy in back_copies(k):
             copy.start()
             backs.append(copy)
+
+    wx[0].wait_recv()
+    wx[4].start()
+    wx[3].wait_recv()
+    wx[5].start()
 
     def trade_copy(k):
         u = up_y(k) * 2 + other if k else pl.ds(y * 2, 2)
@@ -598,8 +644,8 @@
     sum_n = {n: rs(4, n, 1, y_next) for n in even}
     sum_p = {n: rs(5, n, 3, y_prev) for n in odd}
     settle(2)
-    load_wo[1].wait()
-    share_wo[1].wait_recv()
+    load_wo[5].wait()
+    share_wo[5].wait_recv()
     lhs = gather_rows((2,))
     spread[0].start()
     spread[1].start()
@@ -611,19 +657,19 @@
             first_p[n].start()
     settle(1)
     settle(3)
+    lhs = gather_rows((1, 3))
+    spread[4].start()
+    spread[5].start()
+    for n in range(len(PIECES)):
+        columns((1, 3), lhs, n)
+    settle(0)
     spread[0].wait_recv()
     spread[2].start()
     spread[1].wait_recv()
     spread[3].start()
-    lhs = gather_rows((1, 3))
-    for n in range(len(PIECES)):
-        columns((1, 3), lhs, n)
-        if n % 2 == 0:
-            direct_p[n].start()
-        else:
-            direct_n[n].start()
-    spread[4].start()
-    spread[5].start()
+    for n in even:
+        direct_p[n].start()
+        direct_n[n + 1].start()
     for n in even:
         width = PIECES[n][1]
         first_n[n].wait_recv()
@@ -635,10 +681,15 @@
             rb[3, n + 1, :, 0:width].astype(F32) + rv[1, n // 2, :, 0:width].astype(F32)
         ).astype(BF)
         sum_p[n + 1].start()
-    settle(0)
     lhs = gather_rows((0,))
     for n in range(len(PIECES)):
         columns((0,), lhs, n)
+
+    def whole(parts, r):
+        rows = jnp.concatenate(parts, axis=1)
+        return jnp.dot(rows, wg[pl.ds(r, len(parts) // 2)].reshape(len(parts) * COLS, REST), preferred_element_type=F32)
+
+    gacc[...] = whole([jnp.concatenate([att[i, y * 2], att[i, y * 2 + 1]], axis=0) for i in range(2)], 0)
     spread[5].wait_recv()
     pass_on[0].start()
     spread[4].wait_recv()
@@ -647,16 +698,18 @@
     spread[3].wait_recv()
     pass_on[1].start()
     for n in (1, 2, 4, 5):
-        wgs[n].wait_recv()
+        wy[n].wait_recv()
+        wx[n].wait_recv()
     for copy in pass_on:
         copy.wait_recv()
-    rows = [jnp.concatenate([att[i, y * 2], att[i, y * 2 + 1]], axis=0) for i in range(2)]
-    rows += [jnp.concatenate([attg[0, r, i], attg[1, r, i]], axis=0) for r in (1, 2, 3) for i in range(2)]
-    acc = jnp.dot(jnp.concatenate(rows, axis=1), wg[...].reshape(8 * COLS, REST), preferred_element_type=F32)
+    acc = gacc[...] + whole(
+        [jnp.concatenate([attg[0, r, i], attg[1, r, i]], axis=0) for r in (1, 2, 3) for i in range(2)], 1
+    )
     gout[...] = acc.astype(BF).reshape(2, SHARD, REST)
     give = remote(gout.at[other], gin, give_send, give_recv, partner)
     give.start()
-    mixed_ref[:, own_cols] = gout[c]
+    for there, here in whole_cols(c):
+        mixed_ref[:, there] = gout[c, :, here]
     for n in even:
         direct_n[n + 1].wait_recv()
         direct_p[n].wait_recv()
@@ -667,10 +720,11 @@
         acc = acc + rv[4 if n % 2 == 0 else 5, n // 2, :, 0:width].astype(F32)
         mixed_ref[:, start : start + width] = acc.astype(BF)
     give.wait_recv()
-    mixed_ref[:, other_cols] = gin[...]
+    for there, here in whole_cols(other):
+        mixed_ref[:, there] = gin[:, here]
 
     trades = [trade_copy(k) for k in range(4)]
-    for copy in ag + dd + share_wo + wgs + backs + trades + spread + pass_on + [give]:
+    for copy in ag + dd + share_wo + wq + wy + wx + backs + trades + spread + pass_on + [give]:
         copy.wait_send()
     pl.when(has_after)(halo[0].wait_send)
     pl.when(has_before)(halo[1].wait_send)
@@ -744,12 +798,13 @@
         vm((4, 2, COLS, REST), BF),
         vm((2, SHARD, COLS), BF),
         vm((2, 4, 2, SHARD, COLS), BF),
+        vm((2 * SHARD, REST), F32),
         vm((2, SHARD, REST), BF),
         vm((SHARD, REST), BF),
-        dma((8,)),
+        dma((12,)),
         dma((6,)), dma((6,)),
         dma((7,)), dma((7,)),
-        dma((2,)), dma((2,)),
+        dma((6,)), dma((6,)),
         dma((4, 3, 2)), dma((4, 3, 2)),
         dma((4, 3, 2)), dma((4, 3, 2)),
         dma((4, 2, 4)), dma((4, 2, 4)),
@@ -757,6 +812,7 @@
         dma((4, 3, 2)), dma((4, 3, 2)),
         dma((4,)), dma((4,)),
         dma((6, len(PIECES) // 2)), dma((6, len(PIECES) // 2)),
+        dma((12,)), dma((12,)),
         dma((6,)), dma((6,)),
         dma((6,)), dma((6,)),
         dma((3,)), dma((3,)),

time: 72.7 us -> 70.1 us (0.964)
  Pallas kernels: 71.6 us -> 68.6 us
    pallas_call x1, Pallas kernels: 69.8 us -> 66.8 us  [per_device(): pl.pallas_call(kernel, out_shape=(jax.ShapeDtypeStruct((SHARD, D), BF), j...]
where the time goes in v4:
time: 70.1 us; the launch traced here: 69.4 us
  Pallas kernels  68.6 us (98%)
  between operations  0.8 us (1%)
    pallas_call x1, Pallas kernels, per_device(): pl.pallas_call(kernel, out_shape=(jax.ShapeDtypeStruct((SHARD, D), BF), j...  66.8 us
    pallas_call x1, Pallas kernels, per_device(): pl.pallas_call(hand_on, out_shape=(jax.ShapeDtypeStruct((SHARD, D), BF),...  1.81 us

profile of v4, /device:TPU:1, one launch (start us, length us, event | category | flops | bytes accessed | tf_op | source)
XLA Modules:
  0.0 69.4 jit_solution(3088702077756010800)
XLA Ops:
  0.6 66.8 %shard_map.86 = (bf16[64,4096]{1,0:T(8,128)(2,1)}, f32[4,512]{1,0:T(4,128)}) custom-call(bf16[64,4096]{1,0:T(8,128)(2,1)} %x_hbm.1, bf16[4096,256]{1,0:T(8,128)(2,1)} %wq_hbm.1, bf16[4096,256]{1,0:T(8,128)(2,1)} %wk_hbm.1, bf16[4096,256]{1,0:T(8,128)(2,1)} %wv_hbm.1, bf16[256,4096]{1,0:T(8,128)(2,1)} %wo_hbm.1, f32[2,64,128]{2,1,0:T(8,128)} %constant.4.clone.near_hbm, ...), custom_call_target="tpu_custom_call" | custom-call | tf_op jit(solution)/shard_map/pallas_call | solution.py:823
  67.4 1.8 %shard_map.87 = (bf16[64,4096]{1,0:T(8,128)(2,1)}, f32[4,512]{1,0:T(4,128)}) custom-call(bf16[64,4096]{1,0:T(8,128)(2,1)} %get-tuple-element.4.mixed_in, f32[4,512]{1,0:T(4,128)} %get-tuple-element.5.logw_in), custom_call_target="tpu_custom_call" | custom-call | tf_op jit(solution)/shard_map/pallas_call | solution.py:833

commit v5 on v4

--- a/solution.py
+++ b/solution.py
@@ -14,12 +14,13 @@
 D = 4096
 COLS = 256
 SIDE = 64
-PIECES = ((0, 512), (512, 512), (1024, 384), (1408, 384))
-WIDEST = 512
-RING = 1792
+PIECES = ((0, 384), (384, 384), (768, 384), (1152, 384))
+WIDEST = 384
+RING = 1536
 REST = (D - RING) // 2
 QUARTER = 128
-ALONE = REST - 4 * QUARTER
+PAIR = 128
+ALONE = REST - 4 * QUARTER - 2 * PAIR
 TOKENS = 16384
 ROTARY_BASE = 500000.0
 NEG = -1e30
@@ -96,7 +97,7 @@
     loc_sem, ag_send, ag_recv, dd_send, dd_recv, wo_send, wo_recv,
     xs_send, xs_recv, xq_send, xq_recv, z_send, z_recv, n_send, n_recv, ret_send, ret_recv,
     at_send, at_recv, rs_send, rs_recv,
-    wg_send, wg_recv, wx_send, wx_recv, sp_send, sp_recv, pass_send, pass_recv, give_send, give_recv,
+    wg_send, wg_recv, wx_send, wx_recv, wz_send, wz_recv, sp_send, sp_recv, pass_send, pass_recv, give_send, give_recv,
 ):
     sp = lax.axis_index("sp")
     tp = lax.axis_index("tp")
@@ -141,19 +142,28 @@
         copy.start()
     ring_cols = pl.ds(0, RING)
 
+    def pair_half(r):
+        return pl.ds(ALONE + r * PAIR, PAIR)
+
+    def quarter(r):
+        return pl.ds(ALONE + 2 * PAIR + r * QUARTER, QUARTER)
+
     def whole_cols(core):
         base = RING + core * REST
-        parts = [(pl.ds(pl.multiple_of(base + 4 * QUARTER, 128), ALONE), pl.ds(0, ALONE))]
+        parts = [(pl.ds(pl.multiple_of(base + 4 * QUARTER + 2 * PAIR, 128), ALONE), pl.ds(0, ALONE))]
+        for r in range(2):
+            start = pl.multiple_of(base + 4 * QUARTER + lax.rem(z + r, 2) * PAIR, 128)
+            parts.append((pl.ds(start, PAIR), pair_half(r)))
         for r in range(4):
             start = pl.multiple_of(base + lax.rem(x + r, NX) * QUARTER, 128)
-            parts.append((pl.ds(start, QUARTER), pl.ds(ALONE + r * QUARTER, QUARTER)))
+            parts.append((pl.ds(start, QUARTER), quarter(r)))
         return parts
 
     load_wo = [
         pltpu.make_async_copy(wo_hbm.at[:, there], wg.at[0, c, :, here], loc_sem.at[6 + n])
         for n, (there, here) in enumerate(whole_cols(c))
     ]
-    load_wo.append(pltpu.make_async_copy(wo_hbm.at[:, ring_cols], wo.at[c], loc_sem.at[11]))
+    load_wo.append(pltpu.make_async_copy(wo_hbm.at[:, ring_cols], wo.at[c], loc_sem.at[13]))
     for copy in load_wo:
         copy.start()
     barrier = pltpu.get_barrier_semaphore()
@@ -318,8 +328,8 @@
                 send_kv.at[slot, d - 1, e], kv5.at[2, yc * 2 + half, mine],
                 xs_send.at[slot, d - 1, e], xs_recv.at[slot, d - 1, e], x_peer[d],
             )
+            for e, (yc, half) in enumerate(slots[slot])
             for d in (2, 1, 3)
-            for e, (yc, half) in enumerate(slots[slot])
         ]
 
     def q_copies(slot):
@@ -348,32 +358,34 @@
     def sort_half(zz, yc, half):
         kvb[zz * 4 + yc, half] = jnp.dot(swap_half, kv5[zz, yc * 2 + half], preferred_element_type=F32).astype(BF)
 
-    def z_start(slot):
-        for copy in kv_copies(slot):
-            copy.wait_recv()
-        for copies in z_copies(slot):
+    def z_start(slot, parts=(0, 1)):
+        for e in parts:
+            for copy in kv_copies(slot)[e * 3 : e * 3 + 3]:
+                copy.wait_recv()
+            copies = z_copies(slot)[e]
             pl.when(has_up)(copies[0].start)
             pl.when(has_down)(copies[1].start)
-        for yc, half in slots[slot]:
-            sort_half(2, yc, half)
-
-    def z_forward(slot):
-        for copies in z_copies(slot):
+        for e in parts:
+            sort_half(2, *slots[slot][e])
+
+    def z_forward(slot, parts=(0, 1)):
+        for e in parts:
+            copies = z_copies(slot)[e]
             pl.when(has_down)(copies[0].wait_recv)
             pl.when(has_both)(copies[2].start)
             pl.when(has_up)(copies[1].wait_recv)
             pl.when(has_both)(copies[3].start)
-        for yc, half in slots[slot]:
-            sort_half(1, yc, half)
-            sort_half(3, yc, half)
-
-    def z_finish(slot):
-        for copies in z_copies(slot):
+        for e in parts:
+            sort_half(1, *slots[slot][e])
+            sort_half(3, *slots[slot][e])
+
+    def z_finish(slot, parts=(0, 1)):
+        for e in parts:
+            copies = z_copies(slot)[e]
             pl.when(has_down2)(copies[2].wait_recv)
             pl.when(has_up2)(copies[3].wait_recv)
-        for yc, half in slots[slot]:
-            sort_half(0, yc, half)
-            sort_half(4, yc, half)
+            sort_half(0, *slots[slot][e])
+            sort_half(4, *slots[slot][e])
 
     def q_finish(slot):
         for copy in q_copies(slot):
@@ -400,7 +412,7 @@
         remote(wo_hbm.at[:, there], wg.at[0, c, :, here], wo_send.at[n], wo_recv.at[n], partner)
         for n, (there, here) in enumerate(whole_cols(other))
     ]
-    share_wo.append(remote(wo_hbm.at[:, ring_cols], wo.at[c], wo_send.at[5], wo_recv.at[5], partner))
+    share_wo.append(remote(wo_hbm.at[:, ring_cols], wo.at[c], wo_send.at[7], wo_recv.at[7], partner))
     for copy in share_wo:
         copy.start()
     z_start(0)
@@ -422,6 +434,7 @@
     dd[3].wait_recv()
     dd[4].wait_recv()
     project(2)
+    z_forward(1, (0,))
     ag[4].wait_recv()
     dd[5].start()
     ag[5].wait_recv()
@@ -437,12 +450,10 @@
             )
         ]
 
-    wq = gather_copies(pl.ds(ALONE, QUARTER), 0)
+    wq = gather_copies(quarter(0), 0)
     wy = gather_copies(pl.ds(0, ALONE), 6)
+    wp = gather_copies(pair_half(0), 12)
     others = pl.ds(1, 3)
-
-    def quarter(r):
-        return pl.ds(ALONE + r * QUARTER, QUARTER)
 
     x_next, x_prev = x_peer[1], x_peer[3]
     wx = [
@@ -454,12 +465,17 @@
             ]
         )
     ]
-    for n in range(5):
+    z_pair = ((z + 1 - 2 * lax.rem(z, 2)) * NX + x, tp)
+    wz = [
+        remote(wg.at[others, i, :, pair_half(0)], wg.at[others, i, :, pair_half(1)], wz_send.at[i], wz_recv.at[i], z_pair)
+        for i in range(2)
+    ]
+    for n in range(7):
         load_wo[n].wait()
         share_wo[n].wait_recv()
     for n in (0, 3, 1, 2):
         wq[n].start()
-    z_forward(1)
+    z_forward(1, (1,))
     z_start(2)
     dd[5].wait_recv()
     dd[6].wait_recv()
@@ -475,11 +491,15 @@
     wq[3].wait_recv()
     wq[5].start()
     for n in (0, 3, 1, 2):
-        wy[n].start()
+        wp[n].start()
+    wy[0].start()
+    wy[3].start()
     block1(1)
     block1(2)
-    z_start(3)
-    z_forward(2)
+    z_start(3, (0,))
+    z_forward(2, (0,))
+    z_start(3, (1,))
+    z_forward(2, (1,))
     for n in (1, 2, 4, 5):
         wq[n].wait_recv()
     for n in (0, 3, 1, 2):
@@ -490,7 +510,12 @@
     block1(3)
     for slot in range(4):
         q_finish(slot)
-    z_forward(3)
+    wp[0].wait_recv()
+    wp[4].start()
+    wp[3].wait_recv()
+    wp[5].start()
+    wy[1].start()
+    wy[2].start()
 
     section = iota((1, 384), 1) // 128 - 1
 
@@ -509,21 +534,19 @@
         o8[:, rows, :] = out.reshape(8, 16, COLS)
         l8[:, rows, :] = sums.reshape(8, 16, 128)
 
-    def several(block, count):
-        def body(i, carry):
-            for n in range(count):
-                block(i * count + n)
-            return carry
-
-        return body
-
-    lax.fori_loop(0, 2, several(block8, 2), 0)
-    for slot in range(4):
-        z_finish(slot)
+    block8(1)
+    block8(2)
+    z_forward(3)
+    z_finish(0)
+    z_finish(1)
+    block8(0)
+    block8(3)
+    z_finish(2)
+    z_finish(3, (0,))
 
     def block64(i):
-        half = lax.div(i, 4)
-        rows = pl.ds(pl.multiple_of(lax.rem(i, 4) * 16, 16), 16)
+        half = i // 4
+        rows = slice(i % 4 * 16, i % 4 * 16 + 16)
         q = qb[:, half, rows, :].reshape(64, COLS)
         kv = kvb[:, half, rows, :].reshape(320, 2 * COLS)
         out, sums = attend(q, kv[:, 0:COLS], kv[:, COLS:], bias64[...])
@@ -534,7 +557,17 @@
     wy[4].start()
     wy[3].wait_recv()
     wy[5].start()
-    lax.fori_loop(0, 2, several(block64, 4), 0)
+    for i in range(4):
+        block64(i)
+    z_finish(3, (1,))
+    for i in range(4, 8):
+        block64(i)
+
+
+    for n in (1, 2, 4, 5):
+        wp[n].wait_recv()
+    wz[0].start()
+    wz[1].start()
 
     def join(k):
         i = up_y(k)
@@ -644,8 +677,8 @@
     sum_n = {n: rs(4, n, 1, y_next) for n in even}
     sum_p = {n: rs(5, n, 3, y_prev) for n in odd}
     settle(2)
-    load_wo[5].wait()
-    share_wo[5].wait_recv()
+    load_wo[7].wait()
+    share_wo[7].wait_recv()
     lhs = gather_rows((2,))
     spread[0].start()
     spread[1].start()
@@ -687,24 +720,30 @@
 
     def whole(parts, r):
         rows = jnp.concatenate(parts, axis=1)
-        return jnp.dot(rows, wg[pl.ds(r, len(parts) // 2)].reshape(len(parts) * COLS, REST), preferred_element_type=F32)
+        return jnp.dot(rows, wg[r].reshape(2 * COLS, REST), preferred_element_type=F32)
+
+    def spread_rows(r):
+        return [jnp.concatenate([attg[0, r, i], attg[1, r, i]], axis=0) for i in range(2)]
 
     gacc[...] = whole([jnp.concatenate([att[i, y * 2], att[i, y * 2 + 1]], axis=0) for i in range(2)], 0)
     spread[5].wait_recv()
     pass_on[0].start()
     spread[4].wait_recv()
     pass_on[2].start()
+    for n in (1, 2, 4, 5):
+        wy[n].wait_recv()
+        wx[n].wait_recv()
+    for copy in wz:
+        copy.wait_recv()
     spread[2].wait_recv()
     spread[3].wait_recv()
     pass_on[1].start()
-    for n in (1, 2, 4, 5):
-        wy[n].wait_recv()
-        wx[n].wait_recv()
-    for copy in pass_on:
-        copy.wait_recv()
-    acc = gacc[...] + whole(
-        [jnp.concatenate([attg[0, r, i], attg[1, r, i]], axis=0) for r in (1, 2, 3) for i in range(2)], 1
-    )
+    pass_on[0].wait_recv()
+    gacc[...] += whole(spread_rows(1), 1)
+    pass_on[2].wait_recv()
+    gacc[...] += whole(spread_rows(3), 3)
+    pass_on[1].wait_recv()
+    acc = gacc[...] + whole(spread_rows(2), 2)
     gout[...] = acc.astype(BF).reshape(2, SHARD, REST)
     give = remote(gout.at[other], gin, give_send, give_recv, partner)
     give.start()
@@ -724,7 +763,7 @@
         mixed_ref[:, there] = gin[:, here]
 
     trades = [trade_copy(k) for k in range(4)]
-    for copy in ag + dd + share_wo + wq + wy + wx + backs + trades + spread + pass_on + [give]:
+    for copy in ag + dd + share_wo + wq + wy + wx + wp + wz + backs + trades + spread + pass_on + [give]:
         copy.wait_send()
     pl.when(has_after)(halo[0].wait_send)
     pl.when(has_before)(halo[1].wait_send)
@@ -801,10 +840,10 @@
         vm((2 * SHARD, REST), F32),
         vm((2, SHARD, REST), BF),
         vm((SHARD, REST), BF),
-        dma((12,)),
+        dma((14,)),
         dma((6,)), dma((6,)),
         dma((7,)), dma((7,)),
-        dma((6,)), dma((6,)),
+        dma((8,)), dma((8,)),
         dma((4, 3, 2)), dma((4, 3, 2)),
         dma((4, 3, 2)), dma((4, 3, 2)),
         dma((4, 2, 4)), dma((4, 2, 4)),
@@ -812,8 +851,9 @@
         dma((4, 3, 2)), dma((4, 3, 2)),
         dma((4,)), dma((4,)),
         dma((6, len(PIECES) // 2)), dma((6, len(PIECES) // 2)),
-        dma((12,)), dma((12,)),
+        dma((18,)), dma((18,)),
         dma((6,)), dma((6,)),
+        dma((2,)), dma((2,)),
         dma((6,)), dma((6,)),
         dma((3,)), dma((3,)),
         dma(()), dma(()),

time: 70.1 us -> 69.4 us (0.990)
  no operation moved by 1% of the time
where the time goes in v5:
time: 69.4 us; the launch traced here: 69 us
  Pallas kernels  68.2 us (98%)
  between operations  0.8 us (1%)
    pallas_call x1, Pallas kernels, per_device(): pl.pallas_call(kernel, out_shape=(jax.ShapeDtypeStruct((SHARD, D), BF), j...  66.4 us
    pallas_call x1, Pallas kernels, per_device(): pl.pallas_call(hand_on, out_shape=(jax.ShapeDtypeStruct((SHARD, D), BF),...  1.81 us

profile of v5, /device:TPU:1, one launch (start us, length us, event | category | flops | bytes accessed | tf_op | source)
XLA Modules:
  0.0 69.0 jit_solution(2137474340969335285)
XLA Ops:
  0.6 66.4 %shard_map.86 = (bf16[64,4096]{1,0:T(8,128)(2,1)}, f32[4,512]{1,0:T(4,128)}) custom-call(bf16[64,4096]{1,0:T(8,128)(2,1)} %x_hbm.1, bf16[4096,256]{1,0:T(8,128)(2,1)} %wq_hbm.1, bf16[4096,256]{1,0:T(8,128)(2,1)} %wk_hbm.1, bf16[4096,256]{1,0:T(8,128)(2,1)} %wv_hbm.1, bf16[256,4096]{1,0:T(8,128)(2,1)} %wo_hbm.1, f32[2,64,128]{2,1,0:T(8,128)} %constant.4.clone.near_hbm, ...), custom_call_target="tpu_custom_call" | custom-call | tf_op jit(solution)/shard_map/pallas_call | solution.py:863
  67.0 1.8 %shard_map.87 = (bf16[64,4096]{1,0:T(8,128)(2,1)}, f32[4,512]{1,0:T(4,128)}) custom-call(bf16[64,4096]{1,0:T(8,128)(2,1)} %get-tuple-element.4.mixed_in, f32[4,512]{1,0:T(4,128)} %get-tuple-element.5.logw_in), custom_call_target="tpu_custom_call" | custom-call | tf_op jit(solution)/shard_map/pallas_call | solution.py:873

commit v6 on v5

--- a/solution.py
+++ b/solution.py
@@ -475,6 +475,8 @@
         share_wo[n].wait_recv()
     for n in (0, 3, 1, 2):
         wq[n].start()
+    for n in (0, 3, 1, 2):
+        wp[n].start()
     z_forward(1, (1,))
     z_start(2)
     dd[5].wait_recv()
@@ -490,8 +492,6 @@
     wq[4].start()
     wq[3].wait_recv()
     wq[5].start()
-    for n in (0, 3, 1, 2):
-        wp[n].start()
     wy[0].start()
     wy[3].start()
     block1(1)
@@ -500,14 +500,14 @@
     z_forward(2, (0,))
     z_start(3, (1,))
     z_forward(2, (1,))
+    pl.when(has_before)(halo[0].wait_recv)
+    pl.when(has_after)(halo[1].wait_recv)
+    block1(0)
+    block1(3)
     for n in (1, 2, 4, 5):
         wq[n].wait_recv()
     for n in (0, 3, 1, 2):
         wx[n].start()
-    pl.when(has_before)(halo[0].wait_recv)
-    pl.when(has_after)(halo[1].wait_recv)
-    block1(0)
-    block1(3)
     for slot in range(4):
         q_finish(slot)
     wp[0].wait_recv()
@@ -553,12 +553,12 @@
         ob[:, half, rows, :] = out.astype(BF).reshape(4, 16, COLS)
         lb[:, half, rows, :] = sums.reshape(4, 16, 128)
 
+    for i in range(4):
+        block64(i)
     wy[0].wait_recv()
     wy[4].start()
     wy[3].wait_recv()
     wy[5].start()
-    for i in range(4):
-        block64(i)
     z_finish(3, (1,))
     for i in range(4, 8):
         block64(i)
@@ -749,6 +749,22 @@
     give.start()
     for there, here in whole_cols(c):
         mixed_ref[:, there] = gout[c, :, here]
+    trades = [trade_copy(k) for k in range(4)]
+    for copy in ag + dd + share_wo + wq + wy + wx + wp + wz + backs + trades + spread + pass_on:
+        copy.wait_send()
+    pl.when(has_after)(halo[0].wait_send)
+    pl.when(has_before)(halo[1].wait_send)
+    for group in (first_n, first_p, direct_n, direct_p):
+        for copy in group.values():
+            copy.wait_send()
+    for slot in range(4):
+        for copy in kv_copies(slot) + q_copies(slot):
+            copy.wait_send()
+        for copies in z_copies(slot):
+            pl.when(has_up)(copies[0].wait_send)
+            pl.when(has_down)(copies[1].wait_send)
+            pl.when(has_both)(copies[2].wait_send)
+            pl.when(has_both)(copies[3].wait_send)
     for n in even:
         direct_n[n + 1].wait_recv()
         direct_p[n].wait_recv()
@@ -762,22 +778,10 @@
     for there, here in whole_cols(other):
         mixed_ref[:, there] = gin[:, here]
 
-    trades = [trade_copy(k) for k in range(4)]
-    for copy in ag + dd + share_wo + wq + wy + wx + wp + wz + backs + trades + spread + pass_on + [give]:
-        copy.wait_send()
-    pl.when(has_after)(halo[0].wait_send)
-    pl.when(has_before)(halo[1].wait_send)
-    for group in (first_n, first_p, direct_n, direct_p, sum_n, sum_p):
+    for group in (sum_n, sum_p):
         for copy in group.values():
             copy.wait_send()
-    for slot in range(4):
-        for copy in kv_copies(slot) + q_copies(slot):
-            copy.wait_send()
-        for copies in z_copies(slot):
-            pl.when(has_up)(copies[0].wait_send)
-            pl.when(has_down)(copies[1].wait_send)
-            pl.when(has_both)(copies[2].wait_send)
-            pl.when(has_both)(copies[3].wait_send)
+    give.wait_send()
 
 
 def hand_on(mixed_in, logw_in, mixed_out, logw_out, mixed_vm, logw_vm, sems):

time: 69.4 us -> 69.1 us (level)
  no operation moved by 1% of the time
where the time goes in v6:
time: 69.1 us; the launch traced here: 68.7 us
  Pallas kernels  67.9 us (98%)
  between operations  0.8 us (1%)
    pallas_call x1, Pallas kernels, per_device(): pl.pallas_call(kernel, out_shape=(jax.ShapeDtypeStruct((SHARD, D), BF), j...  66.1 us
    pallas_call x1, Pallas kernels, per_device(): pl.pallas_call(hand_on, out_shape=(jax.ShapeDtypeStruct((SHARD, D), BF),...  1.81 us

profile of v6, /device:TPU:1, one launch (start us, length us, event | category | flops | bytes accessed | tf_op | source)
XLA Modules:
  0.0 68.7 jit_solution(13967413587356517836)
XLA Ops:
  0.6 66.1 %shard_map.86 = (bf16[64,4096]{1,0:T(8,128)(2,1)}, f32[4,512]{1,0:T(4,128)}) custom-call(bf16[64,4096]{1,0:T(8,128)(2,1)} %x_hbm.1, bf16[4096,256]{1,0:T(8,128)(2,1)} %wq_hbm.1, bf16[4096,256]{1,0:T(8,128)(2,1)} %wk_hbm.1, bf16[4096,256]{1,0:T(8,128)(2,1)} %wv_hbm.1, bf16[256,4096]{1,0:T(8,128)(2,1)} %wo_hbm.1, f32[2,64,128]{2,1,0:T(8,128)} %constant.4.clone.near_hbm, ...), custom_call_target="tpu_custom_call" | custom-call | tf_op jit(solution)/shard_map/pallas_call | solution.py:867
  66.7 1.8 %shard_map.87 = (bf16[64,4096]{1,0:T(8,128)(2,1)}, f32[4,512]{1,0:T(4,128)}) custom-call(bf16[64,4096]{1,0:T(8,128)(2,1)} %get-tuple-element.4.mixed_in, f32[4,512]{1,0:T(4,128)} %get-tuple-element.5.logw_in), custom_call_target="tpu_custom_call" | custom-call | tf_op jit(solution)/shard_map/pallas_call | solution.py:877

commit v7 on v6

--- a/solution.py
+++ b/solution.py
@@ -129,6 +129,12 @@
             src_ref=src, dst_ref=dst, send_sem=ssem, recv_sem=rsem, device_id=dev, device_id_type=MESH
         )
 
+    def all_sent(ref, sem):
+        remote(ref, ref, sem, sem, partner).wait_send()
+
+    def all_here(ref, sem):
+        remote(ref, ref, sem, sem, partner).wait_recv()
+
     load_x = pltpu.make_async_copy(x_hbm, xbuf.at[tp], loc_sem.at[0])
     load_x.start()
     loads = [
@@ -181,7 +187,7 @@
     top, low = pl.ds(0, SHARD // 2), pl.ds(SHARD // 2, SHARD // 2)
 
     def shard_copy(i, owner, part, dev):
-        return remote(xbuf.at[owner, part], xbuf.at[owner, part], ag_send.at[i], ag_recv.at[i], dev)
+        return remote(xbuf.at[owner, part], xbuf.at[owner, part], ag_send.at[0], ag_recv.at[i], dev)
 
     own = y * 2 + c
     below = up_y(3) * 2 + c
@@ -199,7 +205,7 @@
 
     def to_partner(i, owner, part=None):
         ref = xbuf.at[owner] if part is None else xbuf.at[owner, part]
-        return remote(ref, ref, dd_send.at[i], dd_recv.at[i], partner)
+        return remote(ref, ref, dd_send.at[0], dd_recv.at[i], partner)
 
     dd = [
         to_partner(0, own),
@@ -326,7 +332,7 @@
         return [
             remote(
                 send_kv.at[slot, d - 1, e], kv5.at[2, yc * 2 + half, mine],
-                xs_send.at[slot, d - 1, e], xs_recv.at[slot, d - 1, e], x_peer[d],
+                xs_send.at[slot], xs_recv.at[slot, e], x_peer[d],
             )
             for e, (yc, half) in enumerate(slots[slot])
             for d in (2, 1, 3)
@@ -336,7 +342,7 @@
         return [
             remote(
                 send_q.at[slot, d - 1, e], qa.at[yc * 2 + half, mine],
-                xq_send.at[slot, d - 1, e], xq_recv.at[slot, d - 1, e], x_peer[d],
+                xq_send.at[slot], xq_recv.at[slot, e], x_peer[d],
             )
             for d in (2, 1, 3)
             for e, (yc, half) in enumerate(slots[slot])
@@ -349,7 +355,7 @@
             route = [(2, 1, z_next), (2, 3, z_prev), (1, 0, z_next), (3, 4, z_prev)]
             out.append(
                 [
-                    remote(kv5.at[a, hc], kv5.at[b, hc], z_send.at[slot, e, i], z_recv.at[slot, e, i], dev)
+                    remote(kv5.at[a, hc], kv5.at[b, hc], z_send.at[i], z_recv.at[slot, e, i], dev)
                     for i, (a, b, dev) in enumerate(route)
                 ]
             )
@@ -360,8 +366,8 @@
 
     def z_start(slot, parts=(0, 1)):
         for e in parts:
-            for copy in kv_copies(slot)[e * 3 : e * 3 + 3]:
-                copy.wait_recv()
+            yc, half = slots[slot][e]
+            all_here(kv5.at[2, yc * 2 + half, pl.ds(0, 48)], xs_recv.at[slot, e])
             copies = z_copies(slot)[e]
             pl.when(has_up)(copies[0].start)
             pl.when(has_down)(copies[1].start)
@@ -388,8 +394,8 @@
             sort_half(4, *slots[slot][e])
 
     def q_finish(slot):
-        for copy in q_copies(slot):
-            copy.wait_recv()
+        for e, (yc, half) in enumerate(slots[slot]):
+            all_here(qa.at[yc * 2 + half, pl.ds(0, 48)], xq_recv.at[slot, e])
         for yc, half in slots[slot]:
             qb[yc, half] = jnp.dot(swap_half, qa[yc * 2 + half], preferred_element_type=F32).astype(BF)
 
@@ -441,7 +447,7 @@
     dd[6].start()
     def gather_copies(cols, first):
         return [
-            remote(wg.at[a, i, :, cols], wg.at[b, i, :, cols], wg_send.at[first + n], wg_recv.at[first + n], dev)
+            remote(wg.at[a, i, :, cols], wg.at[b, i, :, cols], wg_send.at[first // 6], wg_recv.at[first + n], dev)
             for n, (a, b, i, dev) in enumerate(
                 [
                     (0, 3, 0, y_next), (0, 3, 1, y_next), (0, 1, 0, y_prev), (0, 1, 1, y_prev),
@@ -457,7 +463,7 @@
 
     x_next, x_prev = x_peer[1], x_peer[3]
     wx = [
-        remote(wg.at[others, i, :, quarter(a)], wg.at[others, i, :, quarter(b)], wx_send.at[n], wx_recv.at[n], dev)
+        remote(wg.at[others, i, :, quarter(a)], wg.at[others, i, :, quarter(b)], wx_send.at[0], wx_recv.at[n], dev)
         for n, (a, b, i, dev) in enumerate(
             [
                 (0, 3, 0, x_next), (0, 3, 1, x_next), (0, 1, 0, x_prev), (0, 1, 1, x_prev),
@@ -592,8 +598,8 @@
         out = []
         for d in (2, 1, 3):
             to = lax.rem(x + d, NX)
-            out.append(remote(ro.at[k, to], ri.at[k, x], ret_send.at[k, d - 1, 0], ret_recv.at[k, d - 1, 0], x_peer[d]))
-            out.append(remote(rlt.at[k], rit.at[k, x], ret_send.at[k, d - 1, 1], ret_recv.at[k, d - 1, 1], x_peer[d]))
+            out.append(remote(ro.at[k, to], ri.at[k, x], ret_send.at[0], ret_recv.at[k, 0], x_peer[d]))
+            out.append(remote(rlt.at[k], rit.at[k, x], ret_send.at[1], ret_recv.at[k, 1], x_peer[d]))
         return out
 
     backs = []
@@ -628,8 +634,8 @@
 
     def settle(k):
         yc = up_y(k)
-        for copy in back_copies(k):
-            copy.wait_recv()
+        all_here(ri.at[k, pl.ds(0, 3)], ret_recv.at[k, 0])
+        all_here(rit.at[k, pl.ds(0, 3)], ret_recv.at[k, 1])
         for i in range(4):
             o = ri[k, i].astype(F32)
             square[...] = jnp.concatenate([rit[k, i], jnp.zeros((120, 128), F32)], axis=0).T
@@ -665,7 +671,7 @@
     def rs(i, n, src, dev):
         cols = pl.ds(0, PIECES[n][1])
         return remote(
-            rb.at[src, n, :, cols], rv.at[i, n // 2, :, cols], rs_send.at[i, n // 2], rs_recv.at[i, n // 2], dev
+            rb.at[src, n, :, cols], rv.at[i, n // 2, :, cols], rs_send.at[0], rs_recv.at[i, n // 2], dev
         )
 
     even = range(0, len(PIECES), 2)
@@ -749,22 +755,24 @@
     give.start()
     for there, here in whole_cols(c):
         mixed_ref[:, there] = gout[c, :, here]
+    three = pl.ds(0, 3)
+    all_sent(xbuf.at[three], ag_send.at[0])
+    all_sent(xbuf.at[pl.ds(0, 4)], dd_send.at[0])
+    for i, cols in enumerate((quarter(0), pl.ds(0, ALONE), pair_half(0))):
+        all_sent(wg.at[others, both, :, cols], wg_send.at[i])
+    all_sent(wg.at[others, both, :, pl.ds(0, 3 * QUARTER)], wx_send.at[0])
+    all_sent(ro.at[three], ret_send.at[0])
+    all_sent(rit.at[three], ret_send.at[1])
     trades = [trade_copy(k) for k in range(4)]
-    for copy in ag + dd + share_wo + wq + wy + wx + wp + wz + backs + trades + spread + pass_on:
+    for copy in share_wo + wz + trades + spread + pass_on:
         copy.wait_send()
     pl.when(has_after)(halo[0].wait_send)
     pl.when(has_before)(halo[1].wait_send)
-    for group in (first_n, first_p, direct_n, direct_p):
-        for copy in group.values():
-            copy.wait_send()
     for slot in range(4):
-        for copy in kv_copies(slot) + q_copies(slot):
-            copy.wait_send()
-        for copies in z_copies(slot):
-            pl.when(has_up)(copies[0].wait_send)
-            pl.when(has_down)(copies[1].wait_send)
-            pl.when(has_both)(copies[2].wait_send)
-            pl.when(has_both)(copies[3].wait_send)
+        all_sent(send_kv.at[slot], xs_send.at[slot])
+        all_sent(send_q.at[slot], xq_send.at[slot])
+    for i, there in enumerate((has_up, has_down, has_both, has_both)):
+        pl.when(there)(functools.partial(all_sent, kv5.at[0], z_send.at[i]))
     for n in even:
         direct_n[n + 1].wait_recv()
         direct_p[n].wait_recv()
@@ -778,9 +786,7 @@
     for there, here in whole_cols(other):
         mixed_ref[:, there] = gin[:, here]
 
-    for group in (sum_n, sum_p):
-        for copy in group.values():
-            copy.wait_send()
+    all_sent(rb.at[three], rs_send.at[0])
     give.wait_send()
 
 
@@ -845,18 +851,18 @@
         vm((2, SHARD, REST), BF),
         vm((SHARD, REST), BF),
         dma((14,)),
-        dma((6,)), dma((6,)),
-        dma((7,)), dma((7,)),
+        dma((1,)), dma((6,)),
+        dma((1,)), dma((7,)),
         dma((8,)), dma((8,)),
-        dma((4, 3, 2)), dma((4, 3, 2)),
-        dma((4, 3, 2)), dma((4, 3, 2)),
-        dma((4, 2, 4)), dma((4, 2, 4)),
+        dma((4,)), dma((4, 2)),
+        dma((4,)), dma((4, 2)),
+        dma((4,)), dma((4, 2, 4)),
         dma((2,)), dma((2,)),
-        dma((4, 3, 2)), dma((4, 3, 2)),
+        dma((2,)), dma((4, 2)),
         dma((4,)), dma((4,)),
-        dma((6, len(PIECES) // 2)), dma((6, len(PIECES) // 2)),
-        dma((18,)), dma((18,)),
-        dma((6,)), dma((6,)),
+        dma((1,)), dma((6, len(PIECES) // 2)),
+        dma((3,)), dma((18,)),
+        dma((1,)), dma((6,)),
         dma((2,)), dma((2,)),
         dma((6,)), dma((6,)),
         dma((3,)), dma((3,)),

time: 69.1 us -> 67.4 us (0.975)
  Pallas kernels: 67.9 us -> 66.3 us
    pallas_call x1, Pallas kernels: 66.1 us -> 64.5 us  [per_device(): pl.pallas_call(kernel, out_shape=(jax.ShapeDtypeStruct((SHARD, D), BF), j...]
where the time goes in v7:
time: 67.4 us; the launch traced here: 67.1 us
  Pallas kernels  66.3 us (98%)
  between operations  0.8 us (1%)
    pallas_call x1, Pallas kernels, per_device(): pl.pallas_call(kernel, out_shape=(jax.ShapeDtypeStruct((SHARD, D), BF), j...  64.5 us
    pallas_call x1, Pallas kernels, per_device(): pl.pallas_call(hand_on, out_shape=(jax.ShapeDtypeStruct((SHARD, D), BF),...  1.81 us

profile of v7, /device:TPU:1, one launch (start us, length us, event | category | flops | bytes accessed | tf_op | source)
XLA Modules:
  0.0 67.1 jit_solution(14460965456240483269)
XLA Ops:
  0.6 64.5 %shard_map.86 = (bf16[64,4096]{1,0:T(8,128)(2,1)}, f32[4,512]{1,0:T(4,128)}) custom-call(bf16[64,4096]{1,0:T(8,128)(2,1)} %x_hbm.1, bf16[4096,256]{1,0:T(8,128)(2,1)} %wq_hbm.1, bf16[4096,256]{1,0:T(8,128)(2,1)} %wk_hbm.1, bf16[4096,256]{1,0:T(8,128)(2,1)} %wv_hbm.1, bf16[256,4096]{1,0:T(8,128)(2,1)} %wo_hbm.1, f32[2,64,128]{2,1,0:T(8,128)} %constant.4.clone.near_hbm, ...), custom_call_target="tpu_custom_call" | custom-call | tf_op jit(solution)/shard_map/pallas_call | solution.py:873
  65.1 1.8 %shard_map.87 = (bf16[64,4096]{1,0:T(8,128)(2,1)}, f32[4,512]{1,0:T(4,128)}) custom-call(bf16[64,4096]{1,0:T(8,128)(2,1)} %get-tuple-element.4.mixed_in, f32[4,512]{1,0:T(4,128)} %get-tuple-element.5.logw_in), custom_call_target="tpu_custom_call" | custom-call | tf_op jit(solution)/shard_map/pallas_call | solution.py:883

commit v8 on v7

--- a/solution.py
+++ b/solution.py
@@ -21,6 +21,7 @@
 QUARTER = 128
 PAIR = 128
 ALONE = REST - 4 * QUARTER - 2 * PAIR
+TOGETHER = (0, 2, 2, 1, 2, 2)
 TOKENS = 16384
 ROTARY_BASE = 500000.0
 NEG = -1e30
@@ -166,10 +167,10 @@
         return parts
 
     load_wo = [
-        pltpu.make_async_copy(wo_hbm.at[:, there], wg.at[0, c, :, here], loc_sem.at[6 + n])
-        for n, (there, here) in enumerate(whole_cols(c))
-    ]
-    load_wo.append(pltpu.make_async_copy(wo_hbm.at[:, ring_cols], wo.at[c], loc_sem.at[13]))
+        pltpu.make_async_copy(wo_hbm.at[:, there], wg.at[0, c, :, here], loc_sem.at[6])
+        for there, here in whole_cols(c)
+    ]
+    load_wo.append(pltpu.make_async_copy(wo_hbm.at[:, ring_cols], wo.at[c], loc_sem.at[7]))
     for copy in load_wo:
         copy.start()
     barrier = pltpu.get_barrier_semaphore()
@@ -332,7 +333,7 @@
         return [
             remote(
                 send_kv.at[slot, d - 1, e], kv5.at[2, yc * 2 + half, mine],
-                xs_send.at[slot], xs_recv.at[slot, e], x_peer[d],
+                xs_send.at[0], xs_recv.at[slot, e], x_peer[d],
             )
             for e, (yc, half) in enumerate(slots[slot])
             for d in (2, 1, 3)
@@ -342,7 +343,7 @@
         return [
             remote(
                 send_q.at[slot, d - 1, e], qa.at[yc * 2 + half, mine],
-                xq_send.at[slot], xq_recv.at[slot, e], x_peer[d],
+                xq_send.at[0], xq_recv.at[0], x_peer[d],
             )
             for d in (2, 1, 3)
             for e, (yc, half) in enumerate(slots[slot])
@@ -394,8 +395,6 @@
             sort_half(4, *slots[slot][e])
 
     def q_finish(slot):
-        for e, (yc, half) in enumerate(slots[slot]):
-            all_here(qa.at[yc * 2 + half, pl.ds(0, 48)], xq_recv.at[slot, e])
         for yc, half in slots[slot]:
             qb[yc, half] = jnp.dot(swap_half, qa[yc * 2 + half], preferred_element_type=F32).astype(BF)
 
@@ -415,10 +414,10 @@
     dd[0].wait_recv()
     project(0)
     share_wo = [
-        remote(wo_hbm.at[:, there], wg.at[0, c, :, here], wo_send.at[n], wo_recv.at[n], partner)
-        for n, (there, here) in enumerate(whole_cols(other))
-    ]
-    share_wo.append(remote(wo_hbm.at[:, ring_cols], wo.at[c], wo_send.at[7], wo_recv.at[7], partner))
+        remote(wo_hbm.at[:, there], wg.at[0, c, :, here], wo_send.at[0], wo_recv.at[0], partner)
+        for there, here in whole_cols(other)
+    ]
+    share_wo.append(remote(wo_hbm.at[:, ring_cols], wo.at[c], wo_send.at[1], wo_recv.at[1], partner))
     for copy in share_wo:
         copy.start()
     z_start(0)
@@ -447,7 +446,7 @@
     dd[6].start()
     def gather_copies(cols, first):
         return [
-            remote(wg.at[a, i, :, cols], wg.at[b, i, :, cols], wg_send.at[first // 6], wg_recv.at[first + n], dev)
+            remote(wg.at[a, i, :, cols], wg.at[b, i, :, cols], wg_send.at[first // 6], wg_recv.at[first // 6, TOGETHER[n]], dev)
             for n, (a, b, i, dev) in enumerate(
                 [
                     (0, 3, 0, y_next), (0, 3, 1, y_next), (0, 1, 0, y_prev), (0, 1, 1, y_prev),
@@ -460,10 +459,11 @@
     wy = gather_copies(pl.ds(0, ALONE), 6)
     wp = gather_copies(pair_half(0), 12)
     others = pl.ds(1, 3)
+    both = pl.ds(0, 2)
 
     x_next, x_prev = x_peer[1], x_peer[3]
     wx = [
-        remote(wg.at[others, i, :, quarter(a)], wg.at[others, i, :, quarter(b)], wx_send.at[0], wx_recv.at[n], dev)
+        remote(wg.at[others, i, :, quarter(a)], wg.at[others, i, :, quarter(b)], wx_send.at[0], wx_recv.at[TOGETHER[n]], dev)
         for n, (a, b, i, dev) in enumerate(
             [
                 (0, 3, 0, x_next), (0, 3, 1, x_next), (0, 1, 0, x_prev), (0, 1, 1, x_prev),
@@ -476,9 +476,8 @@
         remote(wg.at[others, i, :, pair_half(0)], wg.at[others, i, :, pair_half(1)], wz_send.at[i], wz_recv.at[i], z_pair)
         for i in range(2)
     ]
-    for n in range(7):
-        load_wo[n].wait()
-        share_wo[n].wait_recv()
+    pltpu.make_async_copy(wg.at[0, c], wg.at[0, c], loc_sem.at[6]).wait()
+    all_here(wg.at[0, other], wo_recv.at[0])
     for n in (0, 3, 1, 2):
         wq[n].start()
     for n in (0, 3, 1, 2):
@@ -510,10 +509,10 @@
     pl.when(has_after)(halo[1].wait_recv)
     block1(0)
     block1(3)
-    for n in (1, 2, 4, 5):
-        wq[n].wait_recv()
+    all_here(wg.at[both, both, :, quarter(0)], wg_recv.at[0, 2])
     for n in (0, 3, 1, 2):
         wx[n].start()
+    all_here(qa.at[pl.ds(0, 6)], xq_recv.at[0])
     for slot in range(4):
         q_finish(slot)
     wp[0].wait_recv()
@@ -570,8 +569,7 @@
         block64(i)
 
 
-    for n in (1, 2, 4, 5):
-        wp[n].wait_recv()
+    all_here(wg.at[both, both, :, pair_half(0)], wg_recv.at[2, 2])
     wz[0].start()
     wz[1].start()
 
@@ -618,18 +616,17 @@
         u = up_y(k) * 2 + other if k else pl.ds(y * 2, 2)
         return remote(att.at[c, u], att.at[c, u], at_send.at[k], at_recv.at[k], partner)
 
-    both = pl.ds(0, 2)
     to_far = up_y(2) * 2 + c
     spread = [
         remote(att.at[0, to_far], relay.at[0], sp_send.at[0], sp_recv.at[0], y_next),
-        remote(att.at[1, to_far], relay.at[1], sp_send.at[1], sp_recv.at[1], y_prev),
-        remote(relay.at[0], attg.at[c, 2, 0], sp_send.at[2], sp_recv.at[2], y_next),
-        remote(relay.at[1], attg.at[c, 2, 1], sp_send.at[3], sp_recv.at[3], y_prev),
-        remote(att.at[both, up_y(1) * 2 + c], attg.at[c, 3], sp_send.at[4], sp_recv.at[4], y_next),
-        remote(att.at[both, up_y(3) * 2 + c], attg.at[c, 1], sp_send.at[5], sp_recv.at[5], y_prev),
+        remote(att.at[1, to_far], relay.at[1], sp_send.at[0], sp_recv.at[1], y_prev),
+        remote(relay.at[0], attg.at[c, 2, 0], sp_send.at[0], sp_recv.at[2], y_next),
+        remote(relay.at[1], attg.at[c, 2, 1], sp_send.at[0], sp_recv.at[3], y_prev),
+        remote(att.at[both, up_y(1) * 2 + c], attg.at[c, 3], sp_send.at[0], sp_recv.at[4], y_next),
+        remote(att.at[both, up_y(3) * 2 + c], attg.at[c, 1], sp_send.at[0], sp_recv.at[5], y_prev),
     ]
     pass_on = [
-        remote(attg.at[c, r], attg.at[c, r], pass_send.at[r - 1], pass_recv.at[r - 1], partner) for r in (1, 2, 3)
+        remote(attg.at[c, r], attg.at[c, r], pass_send.at[0], pass_recv.at[r - 1], partner) for r in (1, 2, 3)
     ]
 
     def settle(k):
@@ -736,9 +733,8 @@
     pass_on[0].start()
     spread[4].wait_recv()
     pass_on[2].start()
-    for n in (1, 2, 4, 5):
-        wy[n].wait_recv()
-        wx[n].wait_recv()
+    all_here(wg.at[both, both, :, pl.ds(0, ALONE)], wg_recv.at[1, 2])
+    all_here(wg.at[others, both, :, pl.ds(0, 2 * QUARTER)], wx_recv.at[2])
     for copy in wz:
         copy.wait_recv()
     spread[2].wait_recv()
@@ -764,13 +760,16 @@
     all_sent(ro.at[three], ret_send.at[0])
     all_sent(rit.at[three], ret_send.at[1])
     trades = [trade_copy(k) for k in range(4)]
-    for copy in share_wo + wz + trades + spread + pass_on:
+    all_sent(wg.at[0, other], wo_send.at[0])
+    share_wo[7].wait_send()
+    for copy in wz + trades:
         copy.wait_send()
+    all_sent(attg.at[0], sp_send.at[0])
+    all_sent(attg.at[0, three], pass_send.at[0])
     pl.when(has_after)(halo[0].wait_send)
     pl.when(has_before)(halo[1].wait_send)
-    for slot in range(4):
-        all_sent(send_kv.at[slot], xs_send.at[slot])
-        all_sent(send_q.at[slot], xq_send.at[slot])
+    all_sent(send_kv, xs_send.at[0])
+    all_sent(send_q, xq_send.at[0])
     for i, there in enumerate((has_up, has_down, has_both, has_both)):
         pl.when(there)(functools.partial(all_sent, kv5.at[0], z_send.at[i]))
     for n in even:
@@ -850,22 +849,22 @@
         vm((2 * SHARD, REST), F32),
         vm((2, SHARD, REST), BF),
         vm((SHARD, REST), BF),
-        dma((14,)),
+        dma((8,)),
         dma((1,)), dma((6,)),
         dma((1,)), dma((7,)),
-        dma((8,)), dma((8,)),
-        dma((4,)), dma((4, 2)),
-        dma((4,)), dma((4, 2)),
+        dma((2,)), dma((2,)),
+        dma((1,)), dma((4, 2)),
+        dma((1,)), dma((1,)),
         dma((4,)), dma((4, 2, 4)),
         dma((2,)), dma((2,)),
         dma((2,)), dma((4, 2)),
         dma((4,)), dma((4,)),
         dma((1,)), dma((6, len(PIECES) // 2)),
-        dma((3,)), dma((18,)),
+        dma((3,)), dma((3, 3)),
+        dma((1,)), dma((3,)),
+        dma((2,)), dma((2,)),
         dma((1,)), dma((6,)),
-        dma((2,)), dma((2,)),
-        dma((6,)), dma((6,)),
-        dma((3,)), dma((3,)),
+        dma((1,)), dma((3,)),
         dma(()), dma(()),
     ]
     hbm = pl.BlockSpec(memory_space=pl.ANY)

time: 67.4 us -> 67.1 us (level)
  Pallas kernels: 66.3 us -> 65.4 us
    pallas_call x1, Pallas kernels: 64.5 us -> 63.6 us  [per_device(): pl.pallas_call(kernel, out_shape=(jax.ShapeDtypeStruct((SHARD, D), BF), j...]
where the time goes in v8:
time: 67.1 us; the launch traced here: 66.2 us
  Pallas kernels  65.4 us (97%)
  between operations  0.8 us (1%)
    pallas_call x1, Pallas kernels, per_device(): pl.pallas_call(kernel, out_shape=(jax.ShapeDtypeStruct((SHARD, D), BF), j...  63.6 us
    pallas_call x1, Pallas kernels, per_device(): pl.pallas_call(hand_on, out_shape=(jax.ShapeDtypeStruct((SHARD, D), BF),...  1.81 us

profile of v8, /device:TPU:1, one launch (start us, length us, event | category | flops | bytes accessed | tf_op | source)
XLA Modules:
  0.0 66.2 jit_solution(372786107526355275)
XLA Ops:
  0.6 63.6 %shard_map.86 = (bf16[64,4096]{1,0:T(8,128)(2,1)}, f32[4,512]{1,0:T(4,128)}) custom-call(bf16[64,4096]{1,0:T(8,128)(2,1)} %x_hbm.1, bf16[4096,256]{1,0:T(8,128)(2,1)} %wq_hbm.1, bf16[4096,256]{1,0:T(8,128)(2,1)} %wk_hbm.1, bf16[4096,256]{1,0:T(8,128)(2,1)} %wv_hbm.1, bf16[256,4096]{1,0:T(8,128)(2,1)} %wo_hbm.1, f32[2,64,128]{2,1,0:T(8,128)} %constant.4.clone.near_hbm, ...), custom_call_target="tpu_custom_call" | custom-call | tf_op jit(solution)/shard_map/pallas_call | solution.py:872
  64.2 1.8 %shard_map.87 = (bf16[64,4096]{1,0:T(8,128)(2,1)}, f32[4,512]{1,0:T(4,128)}) custom-call(bf16[64,4096]{1,0:T(8,128)(2,1)} %get-tuple-element.4.mixed_in, f32[4,512]{1,0:T(4,128)} %get-tuple-element.5.logw_in), custom_call_target="tpu_custom_call" | custom-call | tf_op jit(solution)/shard_map/pallas_call | solution.py:882
